TPU v7x, 32 devices: a whole 2x2x4 slice. The times are simulated.
32 devices in a mesh: sp: 8 (over z, y), tp: 4 (over x, core).
Axes of the slice: x: 2, y: 2, z: 4, core: 2. Of those that a mesh axis runs over, the one named last changes fastest.
Arguments:
- stream_in: bfloat16 [2048, 2048], P(('sp', 'tp')), may hold values from -6 to 6
- queries_one: bfloat16 [2048, 1024], P('sp', 'tp'), may hold values from -120 to 120
- queries_two: bfloat16 [2048, 1024], P('sp', 'tp'), may hold values from -120 to 120
- keys_one: bfloat16 [2048, 512], P('sp', 'tp'), may hold values from -7 to 7
- keys_two: bfloat16 [2048, 512], P('sp', 'tp'), may hold values from -7 to 7
- values: bfloat16 [2048, 1024], P('sp', 'tp'), may hold values from -6 to 6
- lambdas: float32 [8], P('tp'), may hold values from 0.3 to 0.8
- head_gain: float32 [256], replicated, may hold values from 0.1 to 1.9
- out_weight: bfloat16 [2048, 2048], P('tp'), may hold values from -0.125 to 0.125
- norm_gain: float32 [2048], replicated, may hold values from 0.1 to 1.9
- expert_ids: int32 [2048, 2], P(('sp', 'tp')), may hold values from 0 to 7, all different within a row; in each aligned block of 64 rows (0 to 63, 64 to 127, ...) at most 32 rows name the same one
- route_weight: float32 [2048, 2], P(('sp', 'tp')), may hold values from 0.1 to 1
- gate_weight: bfloat16 [8, 2048, 1024], P('sp', None, 'tp'), may hold values from -0.125 to 0.125
- up_weight: bfloat16 [8, 2048, 1024], P('sp', None, 'tp'), may hold values from -0.125 to 0.125
- down_weight: bfloat16 [8, 1024, 2048], P('sp', 'tp'), may hold values from -0.1875 to 0.1875
Outputs:
- mixed: bfloat16 [2048, 2048], P(('sp', 'tp'))
Inputs may be any that keep to these rules, and one draw needn't show every extreme that they name: `expert_ids`: each row names 2 different experts. In each aligned block of 64 rows no expert is named more than 32 times, a bound that some block reaches.
All inputs are finite; a program needn't handle non-finite values.
Results may differ from a plain program's by a relative error of at most 0.013.
Values may be sent and summed in bfloat16 or wider, within the bound.
A program may use at most 128 MiB of HBM per device.

v0:
```python
import functools

import jax
import jax.numpy as jnp
from jax import lax
from jax.experimental import pallas as pl
from jax.experimental.pallas import tpu as pltpu
from jax.sharding import PartitionSpec as P

HEAD_DIM = 128
VAL_DIM = 256


EPS = 1e-06
OUT_SCALE = 0.8


MESH = pl.DeviceIdType.MESH
PIECES = 4


def remote(src, dst, send_sem, recv_sem, where):
    return pltpu.make_async_remote_copy(
        src_ref=src,
        dst_ref=dst,
        send_sem=send_sem,
        recv_sem=recv_sem,
        device_id=where,
        device_id_type=MESH,
    )


def greet(devices, count):
    barrier = pltpu.get_barrier_semaphore()
    devices(lambda where: pl.semaphore_signal(barrier, inc=1, device_id=where, device_id_type=MESH))
    pl.semaphore_wait(barrier, count)


def layer_kernel(n, nt, cap, *refs):
    (
        q1_ref, q2_ref, k1_ref, k2_ref, v_ref, lam_ref, gain_ref, ow_ref, stream_ref, norm_ref,
    ) = refs[:10]
    if cap:
        ids_ref, route_ref, gw_ref, uw_ref, dw_ref, out_ref = refs[10:16]
        refs = refs[16:]
    else:
        stream_out, normed_out = refs[10:12]
        refs = refs[12:]
    kv, qs, top, total, acc, heads, ow, near_part, near_got, far_part, far_got = refs[:11]
    local_sem, z_send, z_recv, y_send, y_recv, p_send, p_recv = refs[11:18]
    if cap:
        (
            stream_out, normed_out, gw, uw, dw, blend, blend_hi, blend_lo, send, rows_in, hid, ret, back,
            own_sem, w_send, w_recv, f_send, f_recv, g_send, g_recv, d_send, d_recv, r_send, r_recv,
        ) = refs[18:]

    me, tp = lax.axis_index("sp"), lax.axis_index("tp")
    nz = n // 2
    zi, y = me // 2, lax.rem(me, 2)
    pair = me + 1 - 2 * y
    rows = q1_ref.shape[0]
    hd = HEAD_DIM
    chunk = rows // nt
    side, core = tp // 2, lax.rem(tp, 2)
    near = (me, tp + 1 - 2 * core)
    far = (me, lax.rem(tp + 2, 4))

    loads = [
        pltpu.make_async_copy(k1_ref, kv.at[me, :, pl.ds(0, hd)], local_sem.at[0]),
        pltpu.make_async_copy(k2_ref, kv.at[me, :, pl.ds(hd, hd)], local_sem.at[1]),
        pltpu.make_async_copy(v_ref, kv.at[me, :, pl.ds(2 * hd, VAL_DIM)], local_sem.at[2]),
    ]
    for load in loads:
        load.start()
    if cap:
        ff = gw_ref.shape[2]

        def part_of(i, k):
            if i == 2:
                return dw.at[pl.ds(k * ff, ff), :]
            return (gw, uw)[i].at[:, pl.ds(k * ff, ff)]

        own_loads = [
            pltpu.make_async_copy(ref.at[0], part_of(i, 0), own_sem.at[i])
            for i, ref in enumerate((gw_ref, uw_ref, dw_ref))
        ]
        for load in own_loads:
            load.start()

        def w_copy(i):
            return remote(part_of(i, 0), part_of(i, 1), w_send.at[i], w_recv.at[i], near)

        def piece(p, k):
            if p == 0:
                return part_of(0, k)
            if p <= PIECES:
                deep = gw.shape[0] // PIECES
                return uw.at[pl.ds((p - 1) * deep, deep), pl.ds(k * ff, ff)]
            wide = dw.shape[1] // PIECES
            return dw.at[pl.ds(k * ff, ff), pl.ds((p - 1 - PIECES) * wide, wide)]

        def far_piece(p):
            return remote(piece(p, 0), piece(p, 2), f_send.at[p], f_recv.at[p], far)

        def relay(p):
            return remote(piece(p, 2), piece(p, 3), g_send.at[p], g_recv.at[p], near)

    ow_load = pltpu.make_async_copy(ow_ref, ow, local_sem.at[3])
    ow_load.start()

    def peers(tell):
        def column(s, _):
            @pl.when(s != me)
            def _():
                tell((s, tp))
            return 0
        lax.fori_loop(0, n, column, 0)
        tell(near)
        tell(far)

    greet(peers, n - 1 + 2)
    for load in loads:
        load.wait()

    def hop(z):
        b = 2 * z + y
        return remote(kv.at[b], kv.at[b], z_send.at[z], z_recv.at[z], (lax.rem(me + 2, n), tp))

    def y_copy(z):
        b = 2 * z + y
        return remote(kv.at[b], kv.at[b], y_send.at[z], y_recv.at[z], (pair, tp))

    def y_arrival(z):
        b = 2 * z + 1 - y
        return remote(kv.at[b], kv.at[b], y_send.at[z], y_recv.at[z], (pair, tp))

    @pl.when(zi < nz - 1)
    def _():
        hop(zi).start()

    @pl.when(y == 0)
    def _():
        y_copy(zi).start()

    if cap:
        own_loads[0].wait()
        far_piece(0).start()
        own_loads[1].wait()
        for p in range(1, PIECES - 2):
            far_piece(p).start()
        own_loads[2].wait()
        for i in range(3):
            w_copy(i).start()

    for i, ref in enumerate((q1_ref, q2_ref)):
        for h in range(2):
            qs[i, h * rows:(h + 1) * rows, :] = ref[:, h * hd:(h + 1) * hd]

    scale = HEAD_DIM ** (-0.5)

    def fold(b, first):
        vals = kv[b, :, 2 * hd:]
        for i in range(2):
            keys = kv[b, :, i * hd:(i + 1) * hd]
            s = lax.dot_general(qs[i], keys, (((1,), (1,)), ((), ())), preferred_element_type=jnp.float32)
            if first:
                r = lax.broadcasted_iota(jnp.int32, (2, rows, rows), 1).reshape(2 * rows, rows)
                c = lax.broadcasted_iota(jnp.int32, (2 * rows, rows), 1)
                s = jnp.where(c <= r, s, -jnp.inf)
                new = jnp.max(s, axis=-1, keepdims=True)
            else:
                old = top[i][:, :1]
                new = jnp.maximum(old, jnp.max(s, axis=-1, keepdims=True))
            e = jnp.exp((s - new) * scale)
            part = jnp.sum(e, axis=-1, keepdims=True)
            pv = jnp.dot(e.astype(jnp.bfloat16), vals, preferred_element_type=jnp.float32)
            if first:
                acc[i] = pv
                total[i] = jnp.broadcast_to(part, (2 * rows, 128))
            else:
                alpha = jnp.exp((old - new) * scale)
                acc[i] = acc[i] * alpha + pv
                total[i] = total[i] * alpha + part
            top[i] = jnp.broadcast_to(new, (2 * rows, 128))

    fold(me, True)

    if cap:
        choices, tokens = ids_ref.shape
        which = lax.broadcasted_iota(jnp.int32, (max(n, 8), tokens), 0)
        named = [(ids_ref[k:k + 1, :] == which).astype(jnp.float32) for k in range(choices)]
        before = lax.broadcasted_iota(jnp.int32, (tokens, tokens), 0) < lax.broadcasted_iota(
            jnp.int32, (tokens, tokens), 1
        )
        counts = jnp.dot(
            sum(named).astype(jnp.bfloat16), before.astype(jnp.bfloat16), preferred_element_type=jnp.float32
        )
        place = lax.broadcasted_iota(jnp.int32, (n * cap, tokens), 0)
        chosen = jnp.zeros((n * cap, tokens), jnp.float32)
        weight = jnp.zeros((n * cap, tokens), jnp.float32)
        for k in range(choices):
            rank = jnp.sum(named[k] * counts, axis=0, keepdims=True).astype(jnp.int32)
            hit = (ids_ref[k:k + 1, :] * cap + rank) == place
            chosen = chosen + hit.astype(jnp.float32)
            weight = weight + jnp.where(hit, route_ref[k:k + 1, :], 0.0)
        blend[...] = chosen.astype(jnp.bfloat16)
        weight = weight.T
        coarse = weight.astype(jnp.bfloat16)
        blend_hi[...] = coarse
        blend_lo[...] = (weight - coarse.astype(jnp.float32)).astype(jnp.bfloat16)

    @pl.when(y == 1)
    def _():
        y_arrival(zi).wait_recv()
        fold(pair, False)

    def walk(d, _):
        z = zi - d
        @pl.when(d <= zi)
        def _():
            hop(z).wait_recv()
            y_copy(z).start()
            @pl.when(zi < nz - 1)
            def _():
                hop(z).start()
            fold(2 * z + y, False)
        @pl.when(d > 1)
        def _():
            y_arrival(z + 1).wait_recv()
            fold(2 * (z + 1) + 1 - y, False)
        return 0

    lax.fori_loop(1, jnp.where(zi > 0, zi + 2, 1), walk, 0)

    for h in range(2):
        r = pl.ds(h * rows, rows)
        one = acc[0, r, :] / total[0, r, :1]
        two = acc[1, r, :] / total[1, r, :1]
        diff = one - lam_ref[h] * two
        ms = jnp.mean(diff * diff, axis=-1, keepdims=True)
        heads[:, h * VAL_DIM:(h + 1) * VAL_DIM] = (
            diff * lax.rsqrt(ms + EPS) * gain_ref[...] * OUT_SCALE
        ).astype(jnp.bfloat16)

    ow_load.wait()

    def project(first, second):
        picked = jnp.concatenate(
            [heads[pl.ds(pl.multiple_of(t * chunk, chunk), chunk), :] for t in (first, second)], axis=0
        )
        return jnp.dot(picked, ow[...], preferred_element_type=jnp.float32)

    away = 1 - side
    near_part[...] = project(2 * away + 1 - core, 2 * side + 1 - core).astype(jnp.bfloat16)
    near_copy = remote(near_part, near_got, p_send.at[0], p_recv.at[0], near)
    near_copy.start()
    mine = project(2 * away + core, 2 * side + core)
    near_copy.wait_recv()
    mine = mine + near_got[...].astype(jnp.float32)
    far_part[...] = mine[:chunk].astype(jnp.bfloat16)
    far_copy = remote(far_part, far_got, p_send.at[1], p_recv.at[1], far)
    far_copy.start()
    if cap:
        for p in range(PIECES - 2, 2 * PIECES + 1):
            far_piece(p).start()
    summed = stream_ref[...].astype(jnp.float32) + mine[chunk:]
    far_copy.wait_recv()
    summed = summed + far_got[...].astype(jnp.float32)
    stream_out[...] = summed
    ms = jnp.mean(summed * summed, axis=-1, keepdims=True)
    normed_out[...] = (summed * lax.rsqrt(ms + EPS) * norm_ref[...]).astype(jnp.bfloat16)

    def finish_attention():
        near_copy.wait_send()
        far_copy.wait_send()

        @pl.when(y == 0)
        def _():
            y_copy(zi).wait_send()

        @pl.when(zi < nz - 1)
        def _():
            hop(zi).wait_send()

        def sent(z, _):
            y_copy(z).wait_send()
            @pl.when(zi < nz - 1)
            def _():
                hop(z).wait_send()
            return 0

        lax.fori_loop(0, zi, sent, 0)

    if not cap:
        finish_attention()
        return

    d_model = normed_out.shape[1]

    def d_copy(s):
        return remote(send.at[s], rows_in.at[me], d_send.at[s], d_recv.at[me], (s, tp))

    def d_arrival(s):
        return remote(send.at[s], rows_in.at[s], d_send.at[s], d_recv.at[s], (s, tp))

    wide = d_model // PIECES

    def r_copy(c, s):
        return remote(ret.at[c, s], back.at[c, me], r_send.at[c, s], r_recv.at[c, me], (s, tp))

    def r_arrival(c, s):
        return remote(ret.at[c, s], back.at[c, s], r_send.at[c, s], r_recv.at[c, s], (s, tp))

    def dispatch(d, _):
        z = lax.rem(zi + d, nz)
        base = pl.multiple_of(2 * z * cap, 2 * cap)
        got = jnp.dot(
            blend[pl.ds(base, 2 * cap), :], normed_out[...], preferred_element_type=jnp.float32
        ).astype(jnp.bfloat16)
        for j in range(2):
            s = 2 * z + j
            @pl.when(s != me)
            def _():
                send[s] = got[j * cap:(j + 1) * cap]
                d_copy(s).start()
            @pl.when(s == me)
            def _():
                rows_in[me] = got[j * cap:(j + 1) * cap]
        return 0

    lax.fori_loop(1, nz + 1, dispatch, 0)

    for i in range(3):
        w_copy(i).wait_recv()
    for p in range(PIECES + 1):
        far_piece(p).wait_recv()
        relay(p).start()
    for p in range(PIECES + 1):
        relay(p).wait_recv()

    def work(d, _):
        z = lax.rem(zi + nz - d, nz)
        for j in range(2):
            s = 2 * z + j
            @pl.when(s != me)
            def _():
                d_arrival(s).wait_recv()
        x = rows_in[pl.ds(2 * z, 2)].reshape(2 * cap, d_model)
        gate = jnp.dot(x, gw[...], preferred_element_type=jnp.float32)
        upper = jnp.dot(x, uw[...], preferred_element_type=jnp.float32)
        base = pl.multiple_of(2 * z * cap, 2 * cap)
        hid[pl.ds(base, 2 * cap), :] = (gate / (1.0 + jnp.exp(-gate)) * upper).astype(jnp.bfloat16)
        return 0

    lax.fori_loop(0, nz, work, 0)

    def give_back(c):
        relay(PIECES + 1 + c).wait_recv()
        down = jnp.dot(
            hid[...], dw[:, c * wide:(c + 1) * wide], preferred_element_type=jnp.float32
        ).astype(jnp.bfloat16)
        ret[c] = down.reshape(n, cap, wide)
        back[c, me] = ret[c, me]

        def one(d, _):
            for j in range(2):
                s = 2 * lax.rem(zi + d, nz) + j
                @pl.when(s != me)
                def _():
                    r_copy(c, s).start()
            return 0

        lax.fori_loop(1, nz + 1, one, 0)

    for c in range(PIECES):
        far_piece(PIECES + 1 + c).wait_recv()
        relay(PIECES + 1 + c).start()
        if c > 0:
            give_back(c - 1)
    give_back(PIECES - 1)

    for c in range(PIECES):
        def arrive(s, _):
            @pl.when(s != me)
            def _():
                r_arrival(c, s).wait_recv()
            return 0

        lax.fori_loop(0, n, arrive, 0)
        results = back[c].reshape(n * cap, wide)
        routed = jnp.dot(blend_hi[...], results, preferred_element_type=jnp.float32)
        routed = routed + jnp.dot(blend_lo[...], results, preferred_element_type=jnp.float32)
        cols = slice(c * wide, (c + 1) * wide)
        out_ref[:, cols] = (stream_out[:, cols] + routed).astype(jnp.bfloat16)

    finish_attention()
    for i in range(3):
        w_copy(i).wait_send()
    for p in range(2 * PIECES + 1):
        far_piece(p).wait_send()
        relay(p).wait_send()

    def finish(s, _):
        @pl.when(s != me)
        def _():
            d_copy(s).wait_send()
            for c in range(PIECES):
                r_copy(c, s).wait_send()
        return 0

    lax.fori_loop(0, n, finish, 0)


def layer(n, nt, cap, *args):
    q1, ow, stream_in = args[0], args[7], args[8]
    rows = q1.shape[0]
    tokens, d = stream_in.shape
    vm = pl.BlockSpec(memory_space=pltpu.VMEM)
    hbm = pl.BlockSpec(memory_space=pl.ANY)
    sm = pl.BlockSpec(memory_space=pltpu.SMEM)
    chunk = rows // nt
    dma = pltpu.SemaphoreType.DMA
    bf, f32 = jnp.bfloat16, jnp.float32
    in_specs = [vm, vm, hbm, hbm, hbm, sm, vm, hbm, vm, vm]
    out_shape = (jax.ShapeDtypeStruct((tokens, d), f32), jax.ShapeDtypeStruct((tokens, d), bf))
    out_specs = (vm, vm)
    scratch = [
        pltpu.VMEM((n, rows, 2 * HEAD_DIM + VAL_DIM), bf),
        pltpu.VMEM((2, 2 * rows, HEAD_DIM), bf),
        pltpu.VMEM((2, 2 * rows, 128), f32),
        pltpu.VMEM((2, 2 * rows, 128), f32),
        pltpu.VMEM((2, 2 * rows, VAL_DIM), f32),
        pltpu.VMEM((rows, 2 * VAL_DIM), bf),
        pltpu.VMEM(ow.shape, bf),
        pltpu.VMEM((2 * chunk, d), bf),
        pltpu.VMEM((2 * chunk, d), bf),
        pltpu.VMEM((chunk, d), bf),
        pltpu.VMEM((chunk, d), bf),
        dma((4,)), dma((n // 2,)), dma((n // 2,)), dma((n // 2,)), dma((n // 2,)), dma((2,)), dma((2,)),
    ]
    if cap:
        ff = args[12].shape[2]
        in_specs = in_specs + [vm, vm, hbm, hbm, hbm]
        out_shape = jax.ShapeDtypeStruct((tokens, d), bf)
        out_specs = vm
        scratch = scratch + [
            pltpu.VMEM((tokens, d), f32),
            pltpu.VMEM((tokens, d), bf),
            pltpu.VMEM((d, nt * ff), bf),
            pltpu.VMEM((d, nt * ff), bf),
            pltpu.VMEM((nt * ff, d), bf),
            pltpu.VMEM((n * cap, tokens), bf),
            pltpu.VMEM((tokens, n * cap), bf),
            pltpu.VMEM((tokens, n * cap), bf),
        ] + [pltpu.VMEM((n, cap, d), bf)] * 2 + [
            pltpu.VMEM((n * cap, nt * ff), bf),
            pltpu.VMEM((PIECES, n, cap, d // PIECES), bf),
            pltpu.VMEM((PIECES, n, cap, d // PIECES), bf),
            dma((3,)), dma((3,)), dma((3,)),
        ] + [dma((2 * PIECES + 1,))] * 4 + [dma((n,))] * 2 + [dma((PIECES, n))] * 2
    return pl.pallas_call(
        functools.partial(layer_kernel, n, nt, cap),
        out_shape=out_shape,
        in_specs=in_specs,
        out_specs=out_specs,
        scratch_shapes=scratch,
        compiler_params=pltpu.CompilerParams(
            collective_id=0, has_side_effects=True, vmem_limit_bytes=58 * 2**20
        ),
        name="layer",
    )(*args)


def shards(
    stream_in,
    queries_one,
    queries_two,
    keys_one,
    keys_two,
    values,
    lambdas,
    head_gain,
    out_weight,
    norm_gain,
    expert_ids,
    route_weight,
    gate_weight,
    up_weight,
    down_weight,
):
    n, nt = lax.axis_size("sp"), lax.axis_size("tp")
    rows_here = stream_in.shape[0]
    top_count = expert_ids.shape[1]
    slot_cap = 2 * top_count * rows_here // n
    shared = (
        queries_one, queries_two, keys_one, keys_two, values, lambdas,
        head_gain.reshape(1, -1), out_weight, stream_in, norm_gain.reshape(1, -1),
    )
    if slot_cap % 16 == 0:
        return layer(
            n, nt, slot_cap, *shared, expert_ids.T, route_weight.T, gate_weight, up_weight, down_weight
        )
    stream, normed = layer(n, nt, 0, *shared)
    flat_ids = expert_ids.reshape(-1)
    count = flat_ids.shape[0]
    order = lax.iota(jnp.int32, count)
    earlier = (flat_ids[None, :] == flat_ids[:, None]) & (order[None, :] < order[:, None])
    ranks = jnp.sum(earlier.astype(jnp.int32), axis=1)
    slots = flat_ids * slot_cap + ranks
    slot_of = slots.reshape(rows_here, top_count)
    places = lax.iota(jnp.int32, n * slot_cap)
    selector = sum(
        (slot_of[:, k][None, :] == places[:, None]).astype(jnp.bfloat16) for k in range(top_count)
    )
    send_rows = jnp.dot(selector, normed, preferred_element_type=jnp.float32).astype(jnp.bfloat16)
    received = lax.all_to_all(send_rows, "sp", split_axis=0, concat_axis=0, tiled=True)
    picked_rows = lax.all_gather(received, "tp", axis=0, tiled=True)
    gate = jnp.dot(picked_rows, gate_weight[0], preferred_element_type=jnp.float32)
    upper = jnp.dot(picked_rows, up_weight[0], preferred_element_type=jnp.float32)
    hidden = (jax.nn.silu(gate) * upper).astype(jnp.bfloat16)
    summed = lax.psum_scatter(
        jnp.dot(hidden, down_weight[0], preferred_element_type=jnp.float32).astype(jnp.bfloat16),
        "tp",
        scatter_dimension=0,
        tiled=True,
    )
    returned = lax.all_to_all(summed, "sp", split_axis=0, concat_axis=0, tiled=True)
    picked = jnp.take(returned, slots, axis=0).reshape(rows_here, top_count, -1).astype(jnp.float32)
    routed = jnp.sum(picked * route_weight[:, :, None], axis=1)
    return (stream + routed).astype(jnp.bfloat16)


def solution(mesh):
    return jax.shard_map(
        shards,
        mesh=mesh,
        in_specs=(
            P(("sp", "tp"), None),
            P("sp", "tp"),
            P("sp", "tp"),
            P("sp", "tp"),
            P("sp", "tp"),
            P("sp", "tp"),
            P("tp"),
            P(),
            P("tp", None),
            P(),
            P(("sp", "tp"), None),
            P(("sp", "tp"), None),
            P("sp", None, "tp"),
            P("sp", None, "tp"),
            P("sp", "tp", None),
        ),
        out_specs=P(("sp", "tp"), None),
        check_vma=False,
    )
```

profile of v0, /device:TPU:1, one launch (start us, length us, event | category | flops | bytes accessed | tf_op | source)
XLA Modules:
  0.0 97.2 jit_solution(17463515599522587842)
XLA Ops:
  0.0 95.5 %layer.1 = bf16[64,2048]{1,0:T(8,128)(2,1)} custom-call(bf16[256,256]{1,0:T(8,128)(2,1)} %refs_0_.1, bf16[256,256]{1,0:T(8,128)(2,1)} %refs_1_.1, bf16[256,128]{1,0:T(8,128)(2,1)} %refs_2_.1, bf16[256,128]{1,0:T(8,128)(2,1)} %refs_3_.1, bf16[256,256]{1,0:T(8,128)(2,1)} %refs_4_.1, f32[2]{0:T(128)} %refs_5_.1, f32[1,256]{1,0:T(1,128)} %bitcast.5, ...), custom_call_target="tpu_custom_call" | custom-call | tf_op jit(solution)/shard_map/layer/pallas_call | solution.py:461
  95.5 1.7 %copy.17 = bf16[64,2048]{1,0:T(8,128)(2,1)} copy(bf16[64,2048]{1,0:T(8,128)(2,1)} %layer.1) | data formatting | bytes 524288
where the time goes:
time: 98.4 us; the launch traced here: 97.2 us
  Pallas kernels  95.5 us (97%)
  local copies, waits for them, and re-layouts  1.67 us (2%)
    pallas_call x1, Pallas kernels, layer(): pl.pallas_call(functools.partial(layer_kernel, n, nt, cap), out_shape=out...  95.5 us

commit v1 on v0

--- a/solution.py
+++ b/solution.py
@@ -16,7 +16,11 @@
 
 
 MESH = pl.DeviceIdType.MESH
-PIECES = 4
+LOG2E = 1.4426950408889634
+DEEP = 8
+WIDE = 8
+DOWN = ((0, 2), (2, 2), (4, 2), (6, 1), (7, 1))
+PARTS = 4
 
 
 def remote(src, dst, send_sem, recv_sem, where):
@@ -50,7 +54,7 @@
     local_sem, z_send, z_recv, y_send, y_recv, p_send, p_recv = refs[11:18]
     if cap:
         (
-            stream_out, normed_out, gw, uw, dw, blend, blend_hi, blend_lo, send, rows_in, hid, ret, back,
+            stream_out, normed_out, gu, dw, blend, blend_hi, blend_lo, send, rows_in, hid, ret, back,
             own_sem, w_send, w_recv, f_send, f_recv, g_send, g_recv, d_send, d_recv, r_send, r_recv,
         ) = refs[18:]
 
@@ -75,10 +79,13 @@
     if cap:
         ff = gw_ref.shape[2]
 
+        deep = gu.shape[1] // DEEP
+        wide = dw.shape[1] // WIDE
+
         def part_of(i, k):
             if i == 2:
                 return dw.at[pl.ds(k * ff, ff), :]
-            return (gw, uw)[i].at[:, pl.ds(k * ff, ff)]
+            return gu.at[i, :, pl.ds(k * ff, ff)]
 
         own_loads = [
             pltpu.make_async_copy(ref.at[0], part_of(i, 0), own_sem.at[i])
@@ -91,19 +98,32 @@
             return remote(part_of(i, 0), part_of(i, 1), w_send.at[i], w_recv.at[i], near)
 
         def piece(p, k):
-            if p == 0:
-                return part_of(0, k)
-            if p <= PIECES:
-                deep = gw.shape[0] // PIECES
-                return uw.at[pl.ds((p - 1) * deep, deep), pl.ds(k * ff, ff)]
-            wide = dw.shape[1] // PIECES
-            return dw.at[pl.ds(k * ff, ff), pl.ds((p - 1 - PIECES) * wide, wide)]
+            rows_of = pl.ds(pl.multiple_of(lax.rem(p, DEEP) * deep, deep), deep)
+            return gu.at[p // DEEP, rows_of, pl.ds(k * ff, ff)]
 
         def far_piece(p):
             return remote(piece(p, 0), piece(p, 2), f_send.at[p], f_recv.at[p], far)
 
         def relay(p):
             return remote(piece(p, 2), piece(p, 3), g_send.at[p], g_recv.at[p], near)
+
+        def down_piece(j, k):
+            first, count = DOWN[j]
+            return dw.at[pl.ds(k * ff, ff), pl.ds(first * wide, count * wide)]
+
+        def far_down(j):
+            p = 2 * DEEP + j
+            return remote(down_piece(j, 0), down_piece(j, 2), f_send.at[p], f_recv.at[p], far)
+
+        def relay_down(j):
+            p = 2 * DEEP + j
+            return remote(down_piece(j, 2), down_piece(j, 3), g_send.at[p], g_recv.at[p], near)
+
+        ahead = jnp.where(zi == 0, 1, jnp.minimum(3 + 2 * zi, 2 * DEEP))
+
+        def far_some(p, _):
+            far_piece(p).start()
+            return 0
 
     ow_load = pltpu.make_async_copy(ow_ref, ow, local_sem.at[3])
     ow_load.start()
@@ -144,10 +164,8 @@
 
     if cap:
         own_loads[0].wait()
-        far_piece(0).start()
         own_loads[1].wait()
-        for p in range(1, PIECES - 2):
-            far_piece(p).start()
+        lax.fori_loop(0, ahead, far_some, 0)
         own_loads[2].wait()
         for i in range(3):
             w_copy(i).start()
@@ -156,7 +174,7 @@
         for h in range(2):
             qs[i, h * rows:(h + 1) * rows, :] = ref[:, h * hd:(h + 1) * hd]
 
-    scale = HEAD_DIM ** (-0.5)
+    scale = HEAD_DIM ** (-0.5) * LOG2E
 
     def fold(b, first):
         vals = kv[b, :, 2 * hd:]
@@ -171,14 +189,14 @@
             else:
                 old = top[i][:, :1]
                 new = jnp.maximum(old, jnp.max(s, axis=-1, keepdims=True))
-            e = jnp.exp((s - new) * scale)
-            part = jnp.sum(e, axis=-1, keepdims=True)
+            e = jnp.exp2((s - new) * scale)
+            part = sum(e[:, c * 128:(c + 1) * 128] for c in range(rows // 128))
             pv = jnp.dot(e.astype(jnp.bfloat16), vals, preferred_element_type=jnp.float32)
             if first:
                 acc[i] = pv
-                total[i] = jnp.broadcast_to(part, (2 * rows, 128))
+                total[i] = part
             else:
-                alpha = jnp.exp((old - new) * scale)
+                alpha = jnp.exp2((old - new) * scale)
                 acc[i] = acc[i] * alpha + pv
                 total[i] = total[i] * alpha + part
             top[i] = jnp.broadcast_to(new, (2 * rows, 128))
@@ -234,8 +252,8 @@
 
     for h in range(2):
         r = pl.ds(h * rows, rows)
-        one = acc[0, r, :] / total[0, r, :1]
-        two = acc[1, r, :] / total[1, r, :1]
+        one = acc[0, r, :] / jnp.sum(total[0, r, :], axis=-1, keepdims=True)
+        two = acc[1, r, :] / jnp.sum(total[1, r, :], axis=-1, keepdims=True)
         diff = one - lam_ref[h] * two
         ms = jnp.mean(diff * diff, axis=-1, keepdims=True)
         heads[:, h * VAL_DIM:(h + 1) * VAL_DIM] = (
@@ -244,35 +262,58 @@
 
     ow_load.wait()
 
-    def project(first, second):
-        picked = jnp.concatenate(
+    d_model = ow.shape[1]
+    span = d_model // PARTS
+
+    def picked(first, second):
+        return jnp.concatenate(
             [heads[pl.ds(pl.multiple_of(t * chunk, chunk), chunk), :] for t in (first, second)], axis=0
         )
-        return jnp.dot(picked, ow[...], preferred_element_type=jnp.float32)
+
+    def near_copy(q):
+        cols = pl.ds(q * span, span)
+        return remote(near_part.at[:, cols], near_got.at[:, cols], p_send.at[0, q], p_recv.at[0, q], near)
+
+    def far_copy(q):
+        cols = pl.ds(q * span, span)
+        return remote(far_part.at[:, cols], far_got.at[:, cols], p_send.at[1, q], p_recv.at[1, q], far)
 
     away = 1 - side
-    near_part[...] = project(2 * away + 1 - core, 2 * side + 1 - core).astype(jnp.bfloat16)
-    near_copy = remote(near_part, near_got, p_send.at[0], p_recv.at[0], near)
-    near_copy.start()
-    mine = project(2 * away + core, 2 * side + core)
-    near_copy.wait_recv()
-    mine = mine + near_got[...].astype(jnp.float32)
-    far_part[...] = mine[:chunk].astype(jnp.bfloat16)
-    far_copy = remote(far_part, far_got, p_send.at[1], p_recv.at[1], far)
-    far_copy.start()
+    other = picked(2 * away + 1 - core, 2 * side + 1 - core)
+    for q in range(PARTS):
+        cols = slice(q * span, (q + 1) * span)
+        near_part[:, cols] = jnp.dot(
+            other, ow[:, cols], preferred_element_type=jnp.float32
+        ).astype(jnp.bfloat16)
+        near_copy(q).start()
+    own = picked(2 * away + core, 2 * side + core)
+    for q in range(PARTS):
+        cols = slice(q * span, (q + 1) * span)
+        mine = jnp.dot(own, ow[:, cols], preferred_element_type=jnp.float32)
+        near_copy(q).wait_recv()
+        mine = mine + near_got[:, cols].astype(jnp.float32)
+        far_part[:, cols] = mine[:chunk].astype(jnp.bfloat16)
+        far_copy(q).start()
+        stream_out[:, cols] = stream_ref[:, cols].astype(jnp.float32) + mine[chunk:]
     if cap:
-        for p in range(PIECES - 2, 2 * PIECES + 1):
-            far_piece(p).start()
-    summed = stream_ref[...].astype(jnp.float32) + mine[chunk:]
-    far_copy.wait_recv()
-    summed = summed + far_got[...].astype(jnp.float32)
-    stream_out[...] = summed
-    ms = jnp.mean(summed * summed, axis=-1, keepdims=True)
-    normed_out[...] = (summed * lax.rsqrt(ms + EPS) * norm_ref[...]).astype(jnp.bfloat16)
+        lax.fori_loop(ahead, 2 * DEEP, far_some, 0)
+        for j in range(len(DOWN)):
+            far_down(j).start()
+    square = jnp.zeros((chunk, 1), jnp.float32)
+    for q in range(PARTS):
+        cols = slice(q * span, (q + 1) * span)
+        far_copy(q).wait_recv()
+        summed = stream_out[:, cols] + far_got[:, cols].astype(jnp.float32)
+        stream_out[:, cols] = summed
+        square = square + jnp.sum(summed * summed, axis=-1, keepdims=True)
+    normed_out[...] = (
+        stream_out[...] * lax.rsqrt(square * (1.0 / d_model) + EPS) * norm_ref[...]
+    ).astype(jnp.bfloat16)
 
     def finish_attention():
-        near_copy.wait_send()
-        far_copy.wait_send()
+        for q in range(PARTS):
+            near_copy(q).wait_send()
+            far_copy(q).wait_send()
 
         @pl.when(y == 0)
         def _():
@@ -295,21 +336,21 @@
         finish_attention()
         return
 
-    d_model = normed_out.shape[1]
-
     def d_copy(s):
         return remote(send.at[s], rows_in.at[me], d_send.at[s], d_recv.at[me], (s, tp))
 
     def d_arrival(s):
         return remote(send.at[s], rows_in.at[s], d_send.at[s], d_recv.at[s], (s, tp))
 
-    wide = d_model // PIECES
-
-    def r_copy(c, s):
-        return remote(ret.at[c, s], back.at[c, me], r_send.at[c, s], r_recv.at[c, me], (s, tp))
-
-    def r_arrival(c, s):
-        return remote(ret.at[c, s], back.at[c, s], r_send.at[c, s], r_recv.at[c, s], (s, tp))
+    def r_copy(j, s):
+        first, count = DOWN[j]
+        w = pl.ds(first, count)
+        return remote(ret.at[w, s], back.at[w, me], r_send.at[j, s], r_recv.at[j, me], (s, tp))
+
+    def r_arrival(j, s):
+        first, count = DOWN[j]
+        w = pl.ds(first, count)
+        return remote(ret.at[w, s], back.at[w, s], r_send.at[j, s], r_recv.at[j, s], (s, tp))
 
     def dispatch(d, _):
         z = lax.rem(zi + d, nz)
@@ -330,82 +371,107 @@
 
     lax.fori_loop(1, nz + 1, dispatch, 0)
 
+    def pass_on(p, _):
+        far_piece(p).wait_recv()
+        relay(p).start()
+        return 0
+
+    lax.fori_loop(0, DEEP, pass_on, 0)
     for i in range(3):
         w_copy(i).wait_recv()
-    for p in range(PIECES + 1):
-        far_piece(p).wait_recv()
-        relay(p).start()
-    for p in range(PIECES + 1):
-        relay(p).wait_recv()
-
-    def work(d, _):
-        z = lax.rem(zi + nz - d, nz)
+    local = 2 * ff
+
+    def gated(x, cols):
+        gate = jnp.dot(x, gu[0, :, cols], preferred_element_type=jnp.float32)
+        upper = jnp.dot(x, gu[1, :, cols], preferred_element_type=jnp.float32)
+        return (gate / (1.0 + jnp.exp(-gate)) * upper).astype(jnp.bfloat16)
+
+    def work(z, _):
+        lax.fori_loop(DEEP + z * (DEEP // nz), DEEP + (z + 1) * (DEEP // nz), pass_on, 0)
         for j in range(2):
             s = 2 * z + j
             @pl.when(s != me)
             def _():
                 d_arrival(s).wait_recv()
         x = rows_in[pl.ds(2 * z, 2)].reshape(2 * cap, d_model)
-        gate = jnp.dot(x, gw[...], preferred_element_type=jnp.float32)
-        upper = jnp.dot(x, uw[...], preferred_element_type=jnp.float32)
         base = pl.multiple_of(2 * z * cap, 2 * cap)
-        hid[pl.ds(base, 2 * cap), :] = (gate / (1.0 + jnp.exp(-gate)) * upper).astype(jnp.bfloat16)
+        hid[pl.ds(base, 2 * cap), :local] = gated(x, slice(0, local))
         return 0
 
     lax.fori_loop(0, nz, work, 0)
 
-    def give_back(c):
-        relay(PIECES + 1 + c).wait_recv()
+    def relayed(p, _):
+        relay(p).wait_recv()
+        return 0
+
+    lax.fori_loop(0, 2 * DEEP, relayed, 0)
+    hid[:, local:] = gated(rows_in[...].reshape(n * cap, d_model), slice(local, 2 * local))
+
+    def give_back(j):
+        far_down(j).wait_recv()
+        relay_down(j).start()
+        relay_down(j).wait_recv()
+        first, count = DOWN[j]
         down = jnp.dot(
-            hid[...], dw[:, c * wide:(c + 1) * wide], preferred_element_type=jnp.float32
+            hid[...], dw[:, first * wide:(first + count) * wide], preferred_element_type=jnp.float32
         ).astype(jnp.bfloat16)
-        ret[c] = down.reshape(n, cap, wide)
-        back[c, me] = ret[c, me]
+        for c in range(count):
+            ret[first + c] = down[:, c * wide:(c + 1) * wide].reshape(n, cap, wide)
+            back[first + c, me] = ret[first + c, me]
 
         def one(d, _):
-            for j in range(2):
-                s = 2 * lax.rem(zi + d, nz) + j
+            for k in range(2):
+                s = 2 * lax.rem(zi + d, nz) + k
                 @pl.when(s != me)
                 def _():
-                    r_copy(c, s).start()
+                    r_copy(j, s).start()
             return 0
 
         lax.fori_loop(1, nz + 1, one, 0)
 
-    for c in range(PIECES):
-        far_piece(PIECES + 1 + c).wait_recv()
-        relay(PIECES + 1 + c).start()
-        if c > 0:
-            give_back(c - 1)
-    give_back(PIECES - 1)
-
-    for c in range(PIECES):
+    def collect(j):
         def arrive(s, _):
             @pl.when(s != me)
             def _():
-                r_arrival(c, s).wait_recv()
+                r_arrival(j, s).wait_recv()
             return 0
 
         lax.fori_loop(0, n, arrive, 0)
-        results = back[c].reshape(n * cap, wide)
-        routed = jnp.dot(blend_hi[...], results, preferred_element_type=jnp.float32)
-        routed = routed + jnp.dot(blend_lo[...], results, preferred_element_type=jnp.float32)
-        cols = slice(c * wide, (c + 1) * wide)
-        out_ref[:, cols] = (stream_out[:, cols] + routed).astype(jnp.bfloat16)
+        first, count = DOWN[j]
+        for c in range(first, first + count):
+            results = back[c].reshape(n * cap, wide)
+            routed = jnp.dot(blend_hi[...], results, preferred_element_type=jnp.float32)
+            routed = routed + jnp.dot(blend_lo[...], results, preferred_element_type=jnp.float32)
+            cols = slice(c * wide, (c + 1) * wide)
+            out_ref[:, cols] = (stream_out[:, cols] + routed).astype(jnp.bfloat16)
+
+    for j in range(len(DOWN)):
+        give_back(j)
+        if j > 1:
+            collect(j - 2)
+    for j in range(max(len(DOWN) - 2, 0), len(DOWN)):
+        collect(j)
 
     finish_attention()
     for i in range(3):
         w_copy(i).wait_send()
-    for p in range(2 * PIECES + 1):
+
+    def passed(p, _):
         far_piece(p).wait_send()
         relay(p).wait_send()
+        return 0
+
+    lax.fori_loop(0, 2 * DEEP, passed, 0)
+    for j in range(len(DOWN)):
+        far_down(j).wait_send()
+        relay_down(j).wait_send()
 
     def finish(s, _):
         @pl.when(s != me)
         def _():
             d_copy(s).wait_send()
-            for c in range(PIECES):
-                r_copy(c, s).wait_send()
+            for j in range(len(DOWN)):
+                r_copy(j, s).wait_send()
         return 0
 
     lax.fori_loop(0, n, finish, 0)
@@ -436,7 +502,7 @@
         pltpu.VMEM((2 * chunk, d), bf),
         pltpu.VMEM((chunk, d), bf),
         pltpu.VMEM((chunk, d), bf),
-        dma((4,)), dma((n // 2,)), dma((n // 2,)), dma((n // 2,)), dma((n // 2,)), dma((2,)), dma((2,)),
+        dma((4,)), dma((n // 2,)), dma((n // 2,)), dma((n // 2,)), dma((n // 2,)), dma((2, PARTS)), dma((2, PARTS)),
     ]
     if cap:
         ff = args[12].shape[2]
@@ -446,18 +512,17 @@
         scratch = scratch + [
             pltpu.VMEM((tokens, d), f32),
             pltpu.VMEM((tokens, d), bf),
-            pltpu.VMEM((d, nt * ff), bf),
-            pltpu.VMEM((d, nt * ff), bf),
+            pltpu.VMEM((2, d, nt * ff), bf),
             pltpu.VMEM((nt * ff, d), bf),
             pltpu.VMEM((n * cap, tokens), bf),
             pltpu.VMEM((tokens, n * cap), bf),
             pltpu.VMEM((tokens, n * cap), bf),
         ] + [pltpu.VMEM((n, cap, d), bf)] * 2 + [
             pltpu.VMEM((n * cap, nt * ff), bf),
-            pltpu.VMEM((PIECES, n, cap, d // PIECES), bf),
-            pltpu.VMEM((PIECES, n, cap, d // PIECES), bf),
+            pltpu.VMEM((WIDE, n, cap, d // WIDE), bf),
+            pltpu.VMEM((WIDE, n, cap, d // WIDE), bf),
             dma((3,)), dma((3,)), dma((3,)),
-        ] + [dma((2 * PIECES + 1,))] * 4 + [dma((n,))] * 2 + [dma((PIECES, n))] * 2
+        ] + [dma((2 * DEEP + len(DOWN),))] * 4 + [dma((n,))] * 2 + [dma((len(DOWN), n))] * 2
     return pl.pallas_call(
         functools.partial(layer_kernel, n, nt, cap),
         out_shape=out_shape,

time: 98.4 us -> 102 us (1.037)
  Pallas kernels: 95.5 us -> 99.6 us
    pallas_call x1, Pallas kernels: 95.5 us -> 99.6 us  [layer(): pl.pallas_call(functools.partial(layer_kernel, n, nt, cap), out_shape=out...]
where the time goes in v1:
time: 102 us; the launch traced here: 101 us
  Pallas kernels  99.6 us (98%)
  local copies, waits for them, and re-layouts  1.67 us (2%)
    pallas_call x1, Pallas kernels, layer(): pl.pallas_call(functools.partial(layer_kernel, n, nt, cap), out_shape=out...  99.6 us

profile of v1, /device:TPU:1, one launch (start us, length us, event | category | flops | bytes accessed | tf_op | source)
XLA Modules:
  0.0 101.3 jit_solution(13836675361862270870)
XLA Ops:
  0.0 99.6 %layer.1 = bf16[64,2048]{1,0:T(8,128)(2,1)} custom-call(bf16[256,256]{1,0:T(8,128)(2,1)} %refs_0_.1, bf16[256,256]{1,0:T(8,128)(2,1)} %refs_1_.1, bf16[256,128]{1,0:T(8,128)(2,1)} %refs_2_.1, bf16[256,128]{1,0:T(8,128)(2,1)} %refs_3_.1, bf16[256,256]{1,0:T(8,128)(2,1)} %refs_4_.1, f32[2]{0:T(128)} %refs_5_.1, f32[1,256]{1,0:T(1,128)} %bitcast.5, ...), custom_call_target="tpu_custom_call" | custom-call | tf_op jit(solution)/shard_map/layer/pallas_call | solution.py:526
  99.6 1.7 %copy.17 = bf16[64,2048]{1,0:T(8,128)(2,1)} copy(bf16[64,2048]{1,0:T(8,128)(2,1)} %layer.1) | data formatting | bytes 524288

commit v2 on v1

--- a/solution.py
+++ b/solution.py
@@ -17,9 +17,7 @@
 
 MESH = pl.DeviceIdType.MESH
 LOG2E = 1.4426950408889634
-DEEP = 8
-WIDE = 8
-DOWN = ((0, 2), (2, 2), (4, 2), (6, 1), (7, 1))
+PIECES = 8
 PARTS = 4
 
 
@@ -54,8 +52,9 @@
     local_sem, z_send, z_recv, y_send, y_recv, p_send, p_recv = refs[11:18]
     if cap:
         (
-            stream_out, normed_out, gu, dw, blend, blend_hi, blend_lo, send, rows_in, hid, ret, back,
-            own_sem, w_send, w_recv, f_send, f_recv, g_send, g_recv, d_send, d_recv, r_send, r_recv,
+            stream_out, normed_out, gu, dw, blend, blend_hi, blend_lo, send, rows_in, hid_out, hid_in, ret, back,
+            own_sem, w_send, w_recv, f_send, f_recv, g_send, g_recv, d_send, d_recv,
+            a_send, a_recv, h_send, h_recv, r_send, r_recv,
         ) = refs[18:]
 
     me, tp = lax.axis_index("sp"), lax.axis_index("tp")
@@ -68,6 +67,7 @@
     side, core = tp // 2, lax.rem(tp, 2)
     near = (me, tp + 1 - 2 * core)
     far = (me, lax.rem(tp + 2, 4))
+    cross = (me, 3 - tp)
 
     loads = [
         pltpu.make_async_copy(k1_ref, kv.at[me, :, pl.ds(0, hd)], local_sem.at[0]),
@@ -79,27 +79,18 @@
     if cap:
         ff = gw_ref.shape[2]
 
-        deep = gu.shape[1] // DEEP
-        wide = dw.shape[1] // WIDE
-
-        def part_of(i, k):
-            if i == 2:
-                return dw.at[pl.ds(k * ff, ff), :]
-            return gu.at[i, :, pl.ds(k * ff, ff)]
-
+        deep = ff // PIECES
         own_loads = [
-            pltpu.make_async_copy(ref.at[0], part_of(i, 0), own_sem.at[i])
-            for i, ref in enumerate((gw_ref, uw_ref, dw_ref))
+            pltpu.make_async_copy(dw_ref.at[0], dw.at[pl.ds(0, ff), :], own_sem.at[0]),
+            pltpu.make_async_copy(gw_ref.at[0], gu.at[:, pl.ds(0, ff)], own_sem.at[1]),
+            pltpu.make_async_copy(uw_ref.at[0], gu.at[:, pl.ds(ff, ff)], own_sem.at[2]),
         ]
         for load in own_loads:
             load.start()
-
-        def w_copy(i):
-            return remote(part_of(i, 0), part_of(i, 1), w_send.at[i], w_recv.at[i], near)
+        w_copy = remote(dw.at[pl.ds(0, ff), :], dw.at[pl.ds(ff, ff), :], w_send.at[0], w_recv.at[0], near)
 
         def piece(p, k):
-            rows_of = pl.ds(pl.multiple_of(lax.rem(p, DEEP) * deep, deep), deep)
-            return gu.at[p // DEEP, rows_of, pl.ds(k * ff, ff)]
+            return dw.at[pl.ds(pl.multiple_of(k * ff + p * deep, deep), deep), :]
 
         def far_piece(p):
             return remote(piece(p, 0), piece(p, 2), f_send.at[p], f_recv.at[p], far)
@@ -107,19 +98,7 @@
         def relay(p):
             return remote(piece(p, 2), piece(p, 3), g_send.at[p], g_recv.at[p], near)
 
-        def down_piece(j, k):
-            first, count = DOWN[j]
-            return dw.at[pl.ds(k * ff, ff), pl.ds(first * wide, count * wide)]
-
-        def far_down(j):
-            p = 2 * DEEP + j
-            return remote(down_piece(j, 0), down_piece(j, 2), f_send.at[p], f_recv.at[p], far)
-
-        def relay_down(j):
-            p = 2 * DEEP + j
-            return remote(down_piece(j, 2), down_piece(j, 3), g_send.at[p], g_recv.at[p], near)
-
-        ahead = jnp.where(zi == 0, 1, jnp.minimum(3 + 2 * zi, 2 * DEEP))
+        ahead = jnp.minimum(3 + 3 * zi, PIECES)
 
         def far_some(p, _):
             far_piece(p).start()
@@ -137,8 +116,9 @@
         lax.fori_loop(0, n, column, 0)
         tell(near)
         tell(far)
-
-    greet(peers, n - 1 + 2)
+        tell(cross)
+
+    greet(peers, n - 1 + 3)
     for load in loads:
         load.wait()
 
@@ -164,11 +144,8 @@
 
     if cap:
         own_loads[0].wait()
-        own_loads[1].wait()
         lax.fori_loop(0, ahead, far_some, 0)
-        own_loads[2].wait()
-        for i in range(3):
-            w_copy(i).start()
+        w_copy.start()
 
     for i, ref in enumerate((q1_ref, q2_ref)):
         for h in range(2):
@@ -296,9 +273,7 @@
         far_copy(q).start()
         stream_out[:, cols] = stream_ref[:, cols].astype(jnp.float32) + mine[chunk:]
     if cap:
-        lax.fori_loop(ahead, 2 * DEEP, far_some, 0)
-        for j in range(len(DOWN)):
-            far_down(j).start()
+        lax.fori_loop(ahead, PIECES, far_some, 0)
     square = jnp.zeros((chunk, 1), jnp.float32)
     for q in range(PARTS):
         cols = slice(q * span, (q + 1) * span)
@@ -337,20 +312,34 @@
         return
 
     def d_copy(s):
-        return remote(send.at[s], rows_in.at[me], d_send.at[s], d_recv.at[me], (s, tp))
+        return remote(send.at[s], rows_in.at[0, me], d_send.at[s], d_recv.at[me], (s, tp))
 
     def d_arrival(s):
-        return remote(send.at[s], rows_in.at[s], d_send.at[s], d_recv.at[s], (s, tp))
-
-    def r_copy(j, s):
-        first, count = DOWN[j]
-        w = pl.ds(first, count)
-        return remote(ret.at[w, s], back.at[w, me], r_send.at[j, s], r_recv.at[j, me], (s, tp))
-
-    def r_arrival(j, s):
-        first, count = DOWN[j]
-        w = pl.ds(first, count)
-        return remote(ret.at[w, s], back.at[w, s], r_send.at[j, s], r_recv.at[j, s], (s, tp))
+        return remote(send.at[s], rows_in.at[0, s], d_send.at[s], d_recv.at[s], (s, tp))
+
+    def near_rows(s):
+        return remote(rows_in.at[0, s], rows_in.at[1, s], a_send.at[0, s], a_recv.at[0, s], near)
+
+    def far_rows(s):
+        return remote(rows_in.at[0, s], rows_in.at[2, s], a_send.at[1, s], a_recv.at[1, s], far)
+
+    def relay_rows(s):
+        return remote(rows_in.at[2, s], rows_in.at[3, s], a_send.at[2, s], a_recv.at[2, s], near)
+
+    def h_copy(z, k):
+        return remote(
+            hid_out.at[z, k - 1],
+            hid_in.at[z, :, pl.ds(k * ff, ff)],
+            h_send.at[k - 1, z],
+            h_recv.at[k - 1, z],
+            (near, far, cross)[k - 1],
+        )
+
+    def r_copy(s):
+        return remote(ret.at[s], back.at[me], r_send.at[s], r_recv.at[me], (s, tp))
+
+    def r_arrival(s):
+        return remote(ret.at[s], back.at[s], r_send.at[s], r_recv.at[s], (s, tp))
 
     def dispatch(d, _):
         z = lax.rem(zi + d, nz)
@@ -366,7 +355,7 @@
                 d_copy(s).start()
             @pl.when(s == me)
             def _():
-                rows_in[me] = got[j * cap:(j + 1) * cap]
+                rows_in[0, me] = got[j * cap:(j + 1) * cap]
         return 0
 
     lax.fori_loop(1, nz + 1, dispatch, 0)
@@ -376,102 +365,113 @@
         relay(p).start()
         return 0
 
-    lax.fori_loop(0, DEEP, pass_on, 0)
-    for i in range(3):
-        w_copy(i).wait_recv()
-    local = 2 * ff
-
-    def gated(x, cols):
-        gate = jnp.dot(x, gu[0, :, cols], preferred_element_type=jnp.float32)
-        upper = jnp.dot(x, gu[1, :, cols], preferred_element_type=jnp.float32)
-        return (gate / (1.0 + jnp.exp(-gate)) * upper).astype(jnp.bfloat16)
-
-    def work(z, _):
-        lax.fori_loop(DEEP + z * (DEEP // nz), DEEP + (z + 1) * (DEEP // nz), pass_on, 0)
+    def share(z):
         for j in range(2):
             s = 2 * z + j
             @pl.when(s != me)
             def _():
                 d_arrival(s).wait_recv()
-        x = rows_in[pl.ds(2 * z, 2)].reshape(2 * cap, d_model)
-        base = pl.multiple_of(2 * z * cap, 2 * cap)
-        hid[pl.ds(base, 2 * cap), :local] = gated(x, slice(0, local))
-        return 0
-
-    lax.fori_loop(0, nz, work, 0)
+            far_rows(s).start()
+            near_rows(s).start()
+
+    def pass_rows(z):
+        for j in range(2):
+            far_rows(2 * z + j).wait_recv()
+            relay_rows(2 * z + j).start()
+
+    def gated(z):
+        for j in range(2):
+            near_rows(2 * z + j).wait_recv()
+        for j in range(2):
+            relay_rows(2 * z + j).wait_recv()
+        x = rows_in[:, pl.ds(2 * z, 2)].reshape(4 * 2 * cap, d_model)
+        gate = jnp.dot(x, gu[:, :ff], preferred_element_type=jnp.float32)
+        upper = jnp.dot(x, gu[:, ff:], preferred_element_type=jnp.float32)
+        hidden = (gate / (1.0 + jnp.exp(-gate)) * upper).astype(jnp.bfloat16)
+        hid_in[z, :, :ff] = hidden[:2 * cap]
+        for k in range(1, 4):
+            hid_out[z, k - 1] = hidden[2 * k * cap:2 * (k + 1) * cap]
+        for k in (2, 3, 1):
+            h_copy(z, k).start()
+
+    def give_back(z):
+        for k in range(1, 4):
+            h_copy(z, k).wait_recv()
+        down = jnp.dot(hid_in[z], dw[...], preferred_element_type=jnp.float32).astype(jnp.bfloat16)
+        for j in range(2):
+            s = 2 * z + j
+            @pl.when(s != me)
+            def _():
+                ret[s] = down[j * cap:(j + 1) * cap]
+                r_copy(s).start()
+            @pl.when(s == me)
+            def _():
+                back[me] = down[j * cap:(j + 1) * cap]
+
+    lax.fori_loop(0, PIECES // 2, pass_on, 0)
+    share(0)
+    pass_rows(0)
+    own_loads[1].wait()
+    own_loads[2].wait()
+    gated(0)
+    lax.fori_loop(PIECES // 2, PIECES, pass_on, 0)
+    w_copy.wait_recv()
 
     def relayed(p, _):
         relay(p).wait_recv()
         return 0
 
-    lax.fori_loop(0, 2 * DEEP, relayed, 0)
-    hid[:, local:] = gated(rows_in[...].reshape(n * cap, d_model), slice(local, 2 * local))
-
-    def give_back(j):
-        far_down(j).wait_recv()
-        relay_down(j).start()
-        relay_down(j).wait_recv()
-        first, count = DOWN[j]
-        down = jnp.dot(
-            hid[...], dw[:, first * wide:(first + count) * wide], preferred_element_type=jnp.float32
-        ).astype(jnp.bfloat16)
-        for c in range(count):
-            ret[first + c] = down[:, c * wide:(c + 1) * wide].reshape(n, cap, wide)
-            back[first + c, me] = ret[first + c, me]
-
-        def one(d, _):
-            for k in range(2):
-                s = 2 * lax.rem(zi + d, nz) + k
-                @pl.when(s != me)
-                def _():
-                    r_copy(j, s).start()
-            return 0
-
-        lax.fori_loop(1, nz + 1, one, 0)
-
-    def collect(j):
-        def arrive(s, _):
-            @pl.when(s != me)
-            def _():
-                r_arrival(j, s).wait_recv()
-            return 0
-
-        lax.fori_loop(0, n, arrive, 0)
-        first, count = DOWN[j]
-        for c in range(first, first + count):
-            results = back[c].reshape(n * cap, wide)
-            routed = jnp.dot(blend_hi[...], results, preferred_element_type=jnp.float32)
-            routed = routed + jnp.dot(blend_lo[...], results, preferred_element_type=jnp.float32)
-            cols = slice(c * wide, (c + 1) * wide)
-            out_ref[:, cols] = (stream_out[:, cols] + routed).astype(jnp.bfloat16)
-
-    for j in range(len(DOWN)):
-        give_back(j)
-        if j > 1:
-            collect(j - 2)
-    for j in range(max(len(DOWN) - 2, 0), len(DOWN)):
-        collect(j)
+    lax.fori_loop(0, PIECES, relayed, 0)
+
+    def work(z, _):
+        share(z)
+        give_back(z - 1)
+        pass_rows(z)
+        gated(z)
+        return 0
+
+    lax.fori_loop(1, nz, work, 0)
+    give_back(nz - 1)
+
+    def arrive(s, _):
+        @pl.when(s != me)
+        def _():
+            r_arrival(s).wait_recv()
+        return 0
+
+    lax.fori_loop(0, n, arrive, 0)
+    for q in range(PARTS):
+        cols = slice(q * span, (q + 1) * span)
+        results = back[:, :, cols].reshape(n * cap, span)
+        routed = jnp.dot(blend_hi[...], results, preferred_element_type=jnp.float32)
+        routed = routed + jnp.dot(blend_lo[...], results, preferred_element_type=jnp.float32)
+        out_ref[:, cols] = (stream_out[:, cols] + routed).astype(jnp.bfloat16)
 
     finish_attention()
-    for i in range(3):
-        w_copy(i).wait_send()
+    w_copy.wait_send()
 
     def passed(p, _):
         far_piece(p).wait_send()
         relay(p).wait_send()
         return 0
 
-    lax.fori_loop(0, 2 * DEEP, passed, 0)
-    for j in range(len(DOWN)):
-        far_down(j).wait_send()
-        relay_down(j).wait_send()
+    lax.fori_loop(0, PIECES, passed, 0)
+
+    def shared(z, _):
+        for k in range(1, 4):
+            h_copy(z, k).wait_send()
+        return 0
+
+    lax.fori_loop(0, nz, shared, 0)
 
     def finish(s, _):
+        near_rows(s).wait_send()
+        far_rows(s).wait_send()
+        relay_rows(s).wait_send()
         @pl.when(s != me)
         def _():
             d_copy(s).wait_send()
-            for j in range(len(DOWN)):
-                r_copy(j, s).wait_send()
+            r_copy(s).wait_send()
         return 0
 
     lax.fori_loop(0, n, finish, 0)
@@ -512,17 +512,19 @@
         scratch = scratch + [
             pltpu.VMEM((tokens, d), f32),
             pltpu.VMEM((tokens, d), bf),
-            pltpu.VMEM((2, d, nt * ff), bf),
+            pltpu.VMEM((d, 2 * ff), bf),
             pltpu.VMEM((nt * ff, d), bf),
             pltpu.VMEM((n * cap, tokens), bf),
             pltpu.VMEM((tokens, n * cap), bf),
             pltpu.VMEM((tokens, n * cap), bf),
-        ] + [pltpu.VMEM((n, cap, d), bf)] * 2 + [
-            pltpu.VMEM((n * cap, nt * ff), bf),
-            pltpu.VMEM((WIDE, n, cap, d // WIDE), bf),
-            pltpu.VMEM((WIDE, n, cap, d // WIDE), bf),
-            dma((3,)), dma((3,)), dma((3,)),
-        ] + [dma((2 * DEEP + len(DOWN),))] * 4 + [dma((n,))] * 2 + [dma((len(DOWN), n))] * 2
+            pltpu.VMEM((n, cap, d), bf),
+            pltpu.VMEM((4, n, cap, d), bf),
+            pltpu.VMEM((n // 2, 3, 2 * cap, ff), bf),
+            pltpu.VMEM((n // 2, 2 * cap, 4 * ff), bf),
+            pltpu.VMEM((n, cap, d), bf),
+            pltpu.VMEM((n, cap, d), bf),
+            dma((3,)), dma((1,)), dma((1,)),
+        ] + [dma((PIECES,))] * 4 + [dma((n,))] * 2 + [dma((3, n))] * 2 + [dma((3, n // 2))] * 2 + [dma((n,))] * 2
     return pl.pallas_call(
         functools.partial(layer_kernel, n, nt, cap),
         out_shape=out_shape,

time: 102 us -> 104 us (1.020)
  the two profiles are of different devices: /device:TPU:1 before, /device:TPU:31 now
where the time goes in v2:
time: 104 us; the launch traced here: 103 us
  Pallas kernels  102 us (98%)
  local copies, waits for them, and re-layouts  1.67 us (2%)
    pallas_call x1, Pallas kernels, layer(): pl.pallas_call(functools.partial(layer_kernel, n, nt, cap), out_shape=out...  102 us

profile of v2, /device:TPU:31, one launch (start us, length us, event | category | flops | bytes accessed | tf_op | source)
XLA Modules:
  0.0 103.4 jit_solution(14363913270287134479)
XLA Ops:
  0.0 101.7 %layer.1 = bf16[64,2048]{1,0:T(8,128)(2,1)} custom-call(bf16[256,256]{1,0:T(8,128)(2,1)} %refs_0_.1, bf16[256,256]{1,0:T(8,128)(2,1)} %refs_1_.1, bf16[256,128]{1,0:T(8,128)(2,1)} %refs_2_.1, bf16[256,128]{1,0:T(8,128)(2,1)} %refs_3_.1, bf16[256,256]{1,0:T(8,128)(2,1)} %refs_4_.1, f32[2]{0:T(128)} %refs_5_.1, f32[1,256]{1,0:T(1,128)} %bitcast.5, ...), custom_call_target="tpu_custom_call" | custom-call | tf_op jit(solution)/shard_map/layer/pallas_call | solution.py:528
  101.7 1.7 %copy.17 = bf16[64,2048]{1,0:T(8,128)(2,1)} copy(bf16[64,2048]{1,0:T(8,128)(2,1)} %layer.1) | data formatting | bytes 524288

commit v3 on v2

--- a/solution.py
+++ b/solution.py
@@ -18,6 +18,7 @@
 MESH = pl.DeviceIdType.MESH
 LOG2E = 1.4426950408889634
 PIECES = 8
+HALVES = 2
 PARTS = 4
 
 
@@ -122,25 +123,31 @@
     for load in loads:
         load.wait()
 
-    def hop(z):
-        b = 2 * z + y
-        return remote(kv.at[b], kv.at[b], z_send.at[z], z_recv.at[z], (lax.rem(me + 2, n), tp))
-
-    def y_copy(z):
-        b = 2 * z + y
-        return remote(kv.at[b], kv.at[b], y_send.at[z], y_recv.at[z], (pair, tp))
-
-    def y_arrival(z):
-        b = 2 * z + 1 - y
-        return remote(kv.at[b], kv.at[b], y_send.at[z], y_recv.at[z], (pair, tp))
-
-    @pl.when(zi < nz - 1)
-    def _():
-        hop(zi).start()
-
-    @pl.when(y == 0)
-    def _():
-        y_copy(zi).start()
+    part_rows = rows // HALVES
+
+    def block(b, c):
+        return kv.at[b, pl.ds(c * part_rows, part_rows), :]
+
+    def hop(z, c):
+        b, i = 2 * z + y, HALVES * z + c
+        return remote(block(b, c), block(b, c), z_send.at[i], z_recv.at[i], (lax.rem(me + 2, n), tp))
+
+    def y_copy(z, c):
+        b, i = 2 * z + y, HALVES * z + c
+        return remote(block(b, c), block(b, c), y_send.at[i], y_recv.at[i], (pair, tp))
+
+    def y_arrival(z, c):
+        b, i = 2 * z + 1 - y, HALVES * z + c
+        return remote(block(b, c), block(b, c), y_send.at[i], y_recv.at[i], (pair, tp))
+
+    for c in range(HALVES):
+        @pl.when(zi < nz - 1)
+        def _():
+            hop(zi, c).start()
+
+        @pl.when(y == 0)
+        def _():
+            y_copy(zi, c).start()
 
     if cap:
         own_loads[0].wait()
@@ -204,28 +211,25 @@
         blend_hi[...] = coarse
         blend_lo[...] = (weight - coarse.astype(jnp.float32)).astype(jnp.bfloat16)
 
-    @pl.when(y == 1)
-    def _():
-        y_arrival(zi).wait_recv()
-        fold(pair, False)
-
     def walk(d, _):
         z = zi - d
         @pl.when(d <= zi)
         def _():
-            hop(z).wait_recv()
-            y_copy(z).start()
-            @pl.when(zi < nz - 1)
-            def _():
-                hop(z).start()
+            for c in range(HALVES):
+                hop(z, c).wait_recv()
+                y_copy(z, c).start()
+                @pl.when(zi < nz - 1)
+                def _():
+                    hop(z, c).start()
             fold(2 * z + y, False)
-        @pl.when(d > 1)
-        def _():
-            y_arrival(z + 1).wait_recv()
+        @pl.when(jnp.logical_or(d > 1, y == 1))
+        def _():
+            for c in range(HALVES):
+                y_arrival(z + 1, c).wait_recv()
             fold(2 * (z + 1) + 1 - y, False)
         return 0
 
-    lax.fori_loop(1, jnp.where(zi > 0, zi + 2, 1), walk, 0)
+    lax.fori_loop(1, jnp.where(zi + y > 0, zi + 2, 1), walk, 0)
 
     for h in range(2):
         r = pl.ds(h * rows, rows)
@@ -290,19 +294,21 @@
             near_copy(q).wait_send()
             far_copy(q).wait_send()
 
-        @pl.when(y == 0)
-        def _():
-            y_copy(zi).wait_send()
-
-        @pl.when(zi < nz - 1)
-        def _():
-            hop(zi).wait_send()
+        for c in range(HALVES):
+            @pl.when(y == 0)
+            def _():
+                y_copy(zi, c).wait_send()
+
+            @pl.when(zi < nz - 1)
+            def _():
+                hop(zi, c).wait_send()
 
         def sent(z, _):
-            y_copy(z).wait_send()
-            @pl.when(zi < nz - 1)
-            def _():
-                hop(z).wait_send()
+            for c in range(HALVES):
+                y_copy(z, c).wait_send()
+                @pl.when(zi < nz - 1)
+                def _():
+                    hop(z, c).wait_send()
             return 0
 
         lax.fori_loop(0, zi, sent, 0)
@@ -342,7 +348,7 @@
         return remote(ret.at[s], back.at[s], r_send.at[s], r_recv.at[s], (s, tp))
 
     def dispatch(d, _):
-        z = lax.rem(zi + d, nz)
+        z = jnp.where(zi >= nz // 2, d, nz - 1 - d)
         base = pl.multiple_of(2 * z * cap, 2 * cap)
         got = jnp.dot(
             blend[pl.ds(base, 2 * cap), :], normed_out[...], preferred_element_type=jnp.float32
@@ -358,7 +364,7 @@
                 rows_in[0, me] = got[j * cap:(j + 1) * cap]
         return 0
 
-    lax.fori_loop(1, nz + 1, dispatch, 0)
+    lax.fori_loop(0, nz, dispatch, 0)
 
     def pass_on(p, _):
         far_piece(p).wait_recv()
@@ -408,13 +414,14 @@
             def _():
                 back[me] = down[j * cap:(j + 1) * cap]
 
-    lax.fori_loop(0, PIECES // 2, pass_on, 0)
+    early = zi >= nz // 2
     share(0)
-    pass_rows(0)
+    @pl.when(early)
+    def _():
+        share(1)
+    lax.fori_loop(0, PIECES, pass_on, 0)
     own_loads[1].wait()
     own_loads[2].wait()
-    gated(0)
-    lax.fori_loop(PIECES // 2, PIECES, pass_on, 0)
     w_copy.wait_recv()
 
     def relayed(p, _):
@@ -424,14 +431,22 @@
     lax.fori_loop(0, PIECES, relayed, 0)
 
     def work(z, _):
-        share(z)
-        give_back(z - 1)
         pass_rows(z)
         gated(z)
-        return 0
-
-    lax.fori_loop(1, nz, work, 0)
-    give_back(nz - 1)
+        ahead_z = jnp.where(early, z + 2, z + 1)
+        @pl.when(ahead_z < nz)
+        def _():
+            share(ahead_z)
+        behind_z = jnp.where(early, z - 1, z)
+        @pl.when(behind_z >= 0)
+        def _():
+            give_back(behind_z)
+        return 0
+
+    lax.fori_loop(0, nz, work, 0)
+    @pl.when(early)
+    def _():
+        give_back(nz - 1)
 
     def arrive(s, _):
         @pl.when(s != me)
@@ -502,7 +517,7 @@
         pltpu.VMEM((2 * chunk, d), bf),
         pltpu.VMEM((chunk, d), bf),
         pltpu.VMEM((chunk, d), bf),
-        dma((4,)), dma((n // 2,)), dma((n // 2,)), dma((n // 2,)), dma((n // 2,)), dma((2, PARTS)), dma((2, PARTS)),
+        dma((4,)), dma((n // 2 * HALVES,)), dma((n // 2 * HALVES,)), dma((n // 2 * HALVES,)), dma((n // 2 * HALVES,)), dma((2, PARTS)), dma((2, PARTS)),
     ]
     if cap:
         ff = args[12].shape[2]

time: 104 us -> 101 us (0.971)
  the two profiles are of different devices: /device:TPU:31 before, /device:TPU:29 now
where the time goes in v3:
time: 101 us
  Pallas kernels  99.1 us (98%)
  local copies, waits for them, and re-layouts  1.67 us (2%)
    pallas_call x1, Pallas kernels, layer(): pl.pallas_call(functools.partial(layer_kernel, n, nt, cap), out_shape=out...  99.1 us

profile of v3, /device:TPU:29, one launch (start us, length us, event | category | flops | bytes accessed | tf_op | source)
XLA Modules:
  0.0 100.8 jit_solution(15851137368213293324)
XLA Ops:
  0.0 99.1 %layer.1 = bf16[64,2048]{1,0:T(8,128)(2,1)} custom-call(bf16[256,256]{1,0:T(8,128)(2,1)} %refs_0_.1, bf16[256,256]{1,0:T(8,128)(2,1)} %refs_1_.1, bf16[256,128]{1,0:T(8,128)(2,1)} %refs_2_.1, bf16[256,128]{1,0:T(8,128)(2,1)} %refs_3_.1, bf16[256,256]{1,0:T(8,128)(2,1)} %refs_4_.1, f32[2]{0:T(128)} %refs_5_.1, f32[1,256]{1,0:T(1,128)} %bitcast.5, ...), custom_call_target="tpu_custom_call" | custom-call | tf_op jit(solution)/shard_map/layer/pallas_call | solution.py:543
  99.1 1.7 %copy.17 = bf16[64,2048]{1,0:T(8,128)(2,1)} copy(bf16[64,2048]{1,0:T(8,128)(2,1)} %layer.1) | data formatting | bytes 524288

commit v4 on v1

--- a/solution.py
+++ b/solution.py
@@ -21,6 +21,7 @@
 WIDE = 8
 DOWN = ((0, 2), (2, 2), (4, 2), (6, 1), (7, 1))
 PARTS = 4
+HALVES = 2
 
 
 def remote(src, dst, send_sem, recv_sem, where):
@@ -50,13 +51,13 @@
     else:
         stream_out, normed_out = refs[10:12]
         refs = refs[12:]
-    kv, qs, top, total, acc, heads, ow, near_part, near_got, far_part, far_got = refs[:11]
-    local_sem, z_send, z_recv, y_send, y_recv, p_send, p_recv = refs[11:18]
+    kv, qs, top, total, acc, heads, ow, stream, near_part, near_got, far_part, far_got = refs[:12]
+    local_sem, z_send, z_recv, y_send, y_recv, p_send, p_recv = refs[12:19]
     if cap:
         (
             stream_out, normed_out, gu, dw, blend, blend_hi, blend_lo, send, rows_in, hid, ret, back,
-            own_sem, w_send, w_recv, f_send, f_recv, g_send, g_recv, d_send, d_recv, r_send, r_recv,
-        ) = refs[18:]
+            chain, own_sem, w_send, w_recv, f_send, f_recv, g_send, g_recv, d_send, d_recv, r_send, r_recv,
+        ) = refs[19:]
 
     me, tp = lax.axis_index("sp"), lax.axis_index("tp")
     nz = n // 2
@@ -74,8 +75,17 @@
         pltpu.make_async_copy(k2_ref, kv.at[me, :, pl.ds(hd, hd)], local_sem.at[1]),
         pltpu.make_async_copy(v_ref, kv.at[me, :, pl.ds(2 * hd, VAL_DIM)], local_sem.at[2]),
     ]
-    for load in loads:
+    rest = [
+        pltpu.make_async_copy(
+            ref.at[:, pl.ds(h * hd, hd)], qs.at[i, pl.ds(h * rows, rows), :], local_sem.at[4 + 2 * i + h]
+        )
+        for i, ref in enumerate((q1_ref, q2_ref))
+        for h in range(2)
+    ]
+    stream_load = pltpu.make_async_copy(stream_ref, stream, local_sem.at[8])
+    for load in loads + rest:
         load.start()
+    stream_load.start()
     if cap:
         ff = gw_ref.shape[2]
 
@@ -119,7 +129,7 @@
             p = 2 * DEEP + j
             return remote(down_piece(j, 2), down_piece(j, 3), g_send.at[p], g_recv.at[p], near)
 
-        ahead = jnp.where(zi == 0, 1, jnp.minimum(3 + 2 * zi, 2 * DEEP))
+        ahead = jnp.minimum(jnp.where(zi == 0, 3 + y, jnp.where(zi == nz - 1, 9, 4 + 2 * zi)), 2 * DEEP)
 
         def far_some(p, _):
             far_piece(p).start()
@@ -128,39 +138,48 @@
     ow_load = pltpu.make_async_copy(ow_ref, ow, local_sem.at[3])
     ow_load.start()
 
+    below, above = zi > 0, zi < nz - 1
+
     def peers(tell):
-        def column(s, _):
-            @pl.when(s != me)
-            def _():
-                tell((s, tp))
-            return 0
-        lax.fori_loop(0, n, column, 0)
         tell(near)
         tell(far)
-
-    greet(peers, n - 1 + 2)
+        tell((pair, tp))
+        @pl.when(below)
+        def _():
+            tell((me - 2, tp))
+        @pl.when(above)
+        def _():
+            tell((me + 2, tp))
+
+    greet(peers, 3 + below.astype(jnp.int32) + above.astype(jnp.int32))
     for load in loads:
         load.wait()
 
-    def hop(z):
-        b = 2 * z + y
-        return remote(kv.at[b], kv.at[b], z_send.at[z], z_recv.at[z], (lax.rem(me + 2, n), tp))
-
-    def y_copy(z):
-        b = 2 * z + y
-        return remote(kv.at[b], kv.at[b], y_send.at[z], y_recv.at[z], (pair, tp))
-
-    def y_arrival(z):
-        b = 2 * z + 1 - y
-        return remote(kv.at[b], kv.at[b], y_send.at[z], y_recv.at[z], (pair, tp))
-
-    @pl.when(zi < nz - 1)
-    def _():
-        hop(zi).start()
-
-    @pl.when(y == 0)
-    def _():
-        y_copy(zi).start()
+    part_rows = rows // HALVES
+
+    def block(b, c):
+        return kv.at[b, pl.ds(c * part_rows, part_rows), :]
+
+    def hop(z, c):
+        b, i = 2 * z + y, HALVES * z + c
+        return remote(block(b, c), block(b, c), z_send.at[i], z_recv.at[i], (jnp.minimum(me + 2, n - 2 + y), tp))
+
+    def y_copy(z, c):
+        b, i = 2 * z + y, HALVES * z + c
+        return remote(block(b, c), block(b, c), y_send.at[i], y_recv.at[i], (pair, tp))
+
+    def y_arrival(z, c):
+        b, i = 2 * z + 1 - y, HALVES * z + c
+        return remote(block(b, c), block(b, c), y_send.at[i], y_recv.at[i], (pair, tp))
+
+    for c in range(HALVES):
+        @pl.when(zi < nz - 1)
+        def _():
+            hop(zi, c).start()
+
+        @pl.when(y == 0)
+        def _():
+            y_copy(zi, c).start()
 
     if cap:
         own_loads[0].wait()
@@ -170,9 +189,8 @@
         for i in range(3):
             w_copy(i).start()
 
-    for i, ref in enumerate((q1_ref, q2_ref)):
-        for h in range(2):
-            qs[i, h * rows:(h + 1) * rows, :] = ref[:, h * hd:(h + 1) * hd]
+    for load in rest:
+        load.wait()
 
     scale = HEAD_DIM ** (-0.5) * LOG2E
 
@@ -185,23 +203,33 @@
                 r = lax.broadcasted_iota(jnp.int32, (2, rows, rows), 1).reshape(2 * rows, rows)
                 c = lax.broadcasted_iota(jnp.int32, (2 * rows, rows), 1)
                 s = jnp.where(c <= r, s, -jnp.inf)
-                new = jnp.max(s, axis=-1, keepdims=True)
-            else:
-                old = top[i][:, :1]
-                new = jnp.maximum(old, jnp.max(s, axis=-1, keepdims=True))
-            e = jnp.exp2((s - new) * scale)
-            part = sum(e[:, c * 128:(c + 1) * 128] for c in range(rows // 128))
-            pv = jnp.dot(e.astype(jnp.bfloat16), vals, preferred_element_type=jnp.float32)
+            new = jnp.broadcast_to(jnp.max(s, axis=-1, keepdims=True), (2 * rows, 128))
+            if not first:
+                old = top[i]
+                new = jnp.maximum(old, new)
+            terms = [jnp.exp2((s[:, c:c + 128] - new) * scale) for c in range(0, rows, 128)]
+            weights = jnp.concatenate([e.astype(jnp.bfloat16) for e in terms], axis=1)
+            pv = jnp.dot(weights, vals, preferred_element_type=jnp.float32)
             if first:
                 acc[i] = pv
-                total[i] = part
+                total[i] = sum(terms)
             else:
                 alpha = jnp.exp2((old - new) * scale)
-                acc[i] = acc[i] * alpha + pv
-                total[i] = total[i] * alpha + part
-            top[i] = jnp.broadcast_to(new, (2 * rows, 128))
+                for c in range(0, VAL_DIM, 128):
+                    acc[i, :, c:c + 128] = acc[i, :, c:c + 128] * alpha + pv[:, c:c + 128]
+                total[i] = total[i] * alpha + sum(terms)
+            top[i] = new
 
     fold(me, True)
+
+    if cap:
+        for side_sem, source, target, where in ((0, above, below, me - 2), (1, below, above, me + 2)):
+            @pl.when(source)
+            def _():
+                pl.semaphore_wait(chain.at[side_sem], 1)
+            @pl.when(target)
+            def _():
+                pl.semaphore_signal(chain.at[side_sem], inc=1, device_id=(where, tp), device_id_type=MESH)
 
     if cap:
         choices, tokens = ids_ref.shape
@@ -227,28 +255,25 @@
         blend_hi[...] = coarse
         blend_lo[...] = (weight - coarse.astype(jnp.float32)).astype(jnp.bfloat16)
 
-    @pl.when(y == 1)
-    def _():
-        y_arrival(zi).wait_recv()
-        fold(pair, False)
-
     def walk(d, _):
         z = zi - d
         @pl.when(d <= zi)
         def _():
-            hop(z).wait_recv()
-            y_copy(z).start()
-            @pl.when(zi < nz - 1)
-            def _():
-                hop(z).start()
+            for c in range(HALVES):
+                hop(z, c).wait_recv()
+                y_copy(z, c).start()
+                @pl.when(zi < nz - 1)
+                def _():
+                    hop(z, c).start()
             fold(2 * z + y, False)
-        @pl.when(d > 1)
+        @pl.when(jnp.logical_or(d > 1, y == 1))
         def _():
-            y_arrival(z + 1).wait_recv()
+            for c in range(HALVES):
+                y_arrival(z + 1, c).wait_recv()
             fold(2 * (z + 1) + 1 - y, False)
         return 0
 
-    lax.fori_loop(1, jnp.where(zi > 0, zi + 2, 1), walk, 0)
+    lax.fori_loop(1, jnp.where(zi + y > 0, zi + 2, 1), walk, 0)
 
     for h in range(2):
         r = pl.ds(h * rows, rows)
@@ -286,6 +311,7 @@
             other, ow[:, cols], preferred_element_type=jnp.float32
         ).astype(jnp.bfloat16)
         near_copy(q).start()
+    stream_load.wait()
     own = picked(2 * away + core, 2 * side + core)
     for q in range(PARTS):
         cols = slice(q * span, (q + 1) * span)
@@ -294,7 +320,7 @@
         mine = mine + near_got[:, cols].astype(jnp.float32)
         far_part[:, cols] = mine[:chunk].astype(jnp.bfloat16)
         far_copy(q).start()
-        stream_out[:, cols] = stream_ref[:, cols].astype(jnp.float32) + mine[chunk:]
+        stream_out[:, cols] = stream[:, cols].astype(jnp.float32) + mine[chunk:]
     if cap:
         lax.fori_loop(ahead, 2 * DEEP, far_some, 0)
         for j in range(len(DOWN)):
@@ -315,19 +341,21 @@
             near_copy(q).wait_send()
             far_copy(q).wait_send()
 
-        @pl.when(y == 0)
-        def _():
-            y_copy(zi).wait_send()
-
-        @pl.when(zi < nz - 1)
-        def _():
-            hop(zi).wait_send()
+        for c in range(HALVES):
+            @pl.when(y == 0)
+            def _():
+                y_copy(zi, c).wait_send()
+
+            @pl.when(zi < nz - 1)
+            def _():
+                hop(zi, c).wait_send()
 
         def sent(z, _):
-            y_copy(z).wait_send()
-            @pl.when(zi < nz - 1)
-            def _():
-                hop(z).wait_send()
+            for c in range(HALVES):
+                y_copy(z, c).wait_send()
+                @pl.when(zi < nz - 1)
+                def _():
+                    hop(z, c).wait_send()
             return 0
 
         lax.fori_loop(0, zi, sent, 0)
@@ -353,7 +381,7 @@
         return remote(ret.at[w, s], back.at[w, s], r_send.at[j, s], r_recv.at[j, s], (s, tp))
 
     def dispatch(d, _):
-        z = lax.rem(zi + d, nz)
+        z = d
         base = pl.multiple_of(2 * z * cap, 2 * cap)
         got = jnp.dot(
             blend[pl.ds(base, 2 * cap), :], normed_out[...], preferred_element_type=jnp.float32
@@ -369,7 +397,7 @@
                 rows_in[me] = got[j * cap:(j + 1) * cap]
         return 0
 
-    lax.fori_loop(1, nz + 1, dispatch, 0)
+    lax.fori_loop(0, nz, dispatch, 0)
 
     def pass_on(p, _):
         far_piece(p).wait_recv()
@@ -487,7 +515,7 @@
     chunk = rows // nt
     dma = pltpu.SemaphoreType.DMA
     bf, f32 = jnp.bfloat16, jnp.float32
-    in_specs = [vm, vm, hbm, hbm, hbm, sm, vm, hbm, vm, vm]
+    in_specs = [hbm, hbm, hbm, hbm, hbm, sm, vm, hbm, hbm, vm]
     out_shape = (jax.ShapeDtypeStruct((tokens, d), f32), jax.ShapeDtypeStruct((tokens, d), bf))
     out_specs = (vm, vm)
     scratch = [
@@ -498,16 +526,17 @@
         pltpu.VMEM((2, 2 * rows, VAL_DIM), f32),
         pltpu.VMEM((rows, 2 * VAL_DIM), bf),
         pltpu.VMEM(ow.shape, bf),
+        pltpu.VMEM((tokens, d), bf),
         pltpu.VMEM((2 * chunk, d), bf),
         pltpu.VMEM((2 * chunk, d), bf),
         pltpu.VMEM((chunk, d), bf),
         pltpu.VMEM((chunk, d), bf),
-        dma((4,)), dma((n // 2,)), dma((n // 2,)), dma((n // 2,)), dma((n // 2,)), dma((2, PARTS)), dma((2, PARTS)),
+        dma((9,)), dma((n // 2 * HALVES,)), dma((n // 2 * HALVES,)), dma((n // 2 * HALVES,)), dma((n // 2 * HALVES,)), dma((2, PARTS)), dma((2, PARTS)),
     ]
     if cap:
         ff = args[12].shape[2]
         in_specs = in_specs + [vm, vm, hbm, hbm, hbm]
-        out_shape = jax.ShapeDtypeStruct((tokens, d), bf)
+        out_shape = pltpu.VMEM((tokens, d), bf)
         out_specs = vm
         scratch = scratch + [
             pltpu.VMEM((tokens, d), f32),
@@ -521,7 +550,7 @@
             pltpu.VMEM((n * cap, nt * ff), bf),
             pltpu.VMEM((WIDE, n, cap, d // WIDE), bf),
             pltpu.VMEM((WIDE, n, cap, d // WIDE), bf),
-            dma((3,)), dma((3,)), dma((3,)),
+            pltpu.SemaphoreType.REGULAR((2,)), dma((3,)), dma((3,)), dma((3,)),
         ] + [dma((2 * DEEP + len(DOWN),))] * 4 + [dma((n,))] * 2 + [dma((len(DOWN), n))] * 2
     return pl.pallas_call(
         functools.partial(layer_kernel, n, nt, cap),

time: 102 us -> 93.5 us (0.917)
  Pallas kernels: 99.6 us -> 92.6 us
    pallas_call x1, Pallas kernels: 99.6 us -> 92.6 us  [layer(): pl.pallas_call(functools.partial(layer_kernel, n, nt, cap), out_shape=out...]
where the time goes in v4:
time: 93.5 us; the launch traced here: 93.4 us
  Pallas kernels  92.6 us (99%)
    pallas_call x1, Pallas kernels, layer(): pl.pallas_call(functools.partial(layer_kernel, n, nt, cap), out_shape=out...  92.6 us

profile of v4, /device:TPU:1, one launch (start us, length us, event | category | flops | bytes accessed | tf_op | source)
XLA Modules:
  0.0 93.4 jit_solution(10930404583717234291)
XLA Ops:
  0.0 92.6 %layer.1 = bf16[64,2048]{1,0:T(8,128)(2,1)S(1)} custom-call(bf16[256,256]{1,0:T(8,128)(2,1)} %refs_0_.1, bf16[256,256]{1,0:T(8,128)(2,1)} %refs_1_.1, bf16[256,128]{1,0:T(8,128)(2,1)} %refs_2_.1, bf16[256,128]{1,0:T(8,128)(2,1)} %refs_3_.1, bf16[256,256]{1,0:T(8,128)(2,1)} %refs_4_.1, f32[2]{0:T(128)} %refs_5_.1, f32[1,256]{1,0:T(1,128)} %bitcast.5, ...), custom_call_target="tpu_custom_call" | custom-call | tf_op jit(solution)/shard_map/layer/pallas_call | solution.py:555
  92.6 0.7 copy.17

commit v5 on v4

--- a/solution.py
+++ b/solution.py
@@ -19,7 +19,7 @@
 LOG2E = 1.4426950408889634
 DEEP = 8
 WIDE = 8
-DOWN = ((0, 2), (2, 2), (4, 2), (6, 1), (7, 1))
+DOWN = ((0, 1), (1, 1), (2, 1), (3, 1), (4, 1), (5, 1), (6, 1), (7, 1))
 PARTS = 4
 HALVES = 2
 
@@ -55,7 +55,7 @@
     local_sem, z_send, z_recv, y_send, y_recv, p_send, p_recv = refs[12:19]
     if cap:
         (
-            stream_out, normed_out, gu, dw, blend, blend_hi, blend_lo, send, rows_in, hid, ret, back,
+            stream_out, normed_out, gu, dw, blend, blend_back, send, rows_in, hid, ret, back,
             chain, own_sem, w_send, w_recv, f_send, f_recv, g_send, g_recv, d_send, d_recv, r_send, r_recv,
         ) = refs[19:]
 
@@ -105,17 +105,17 @@
             load.start()
 
         def w_copy(i):
-            return remote(part_of(i, 0), part_of(i, 1), w_send.at[i], w_recv.at[i], near)
+            return remote(part_of(i, 0), part_of(i, 1), w_send.at[0], w_recv.at[0], near)
 
         def piece(p, k):
             rows_of = pl.ds(pl.multiple_of(lax.rem(p, DEEP) * deep, deep), deep)
             return gu.at[p // DEEP, rows_of, pl.ds(k * ff, ff)]
 
         def far_piece(p):
-            return remote(piece(p, 0), piece(p, 2), f_send.at[p], f_recv.at[p], far)
+            return remote(piece(p, 0), piece(p, 2), f_send.at[0], f_recv.at[p], far)
 
         def relay(p):
-            return remote(piece(p, 2), piece(p, 3), g_send.at[p], g_recv.at[p], near)
+            return remote(piece(p, 2), piece(p, 3), g_send.at[0], g_recv.at[0], near)
 
         def down_piece(j, k):
             first, count = DOWN[j]
@@ -123,13 +123,15 @@
 
         def far_down(j):
             p = 2 * DEEP + j
-            return remote(down_piece(j, 0), down_piece(j, 2), f_send.at[p], f_recv.at[p], far)
+            return remote(down_piece(j, 0), down_piece(j, 2), f_send.at[0], f_recv.at[p], far)
 
         def relay_down(j):
-            p = 2 * DEEP + j
-            return remote(down_piece(j, 2), down_piece(j, 3), g_send.at[p], g_recv.at[p], near)
-
-        ahead = jnp.minimum(jnp.where(zi == 0, 3 + y, jnp.where(zi == nz - 1, 9, 4 + 2 * zi)), 2 * DEEP)
+            return remote(down_piece(j, 2), down_piece(j, 3), g_send.at[0], g_recv.at[1 + j], near)
+
+        def third(k):
+            return dw.at[pl.ds(k, 3 * ff), :]
+
+        ahead = jnp.minimum(jnp.where(zi == 0, 5, jnp.where(zi == nz - 1, 10, 6 + zi)), 2 * DEEP)
 
         def far_some(p, _):
             far_piece(p).start()
@@ -222,14 +224,16 @@
 
     fold(me, True)
 
-    if cap:
-        for side_sem, source, target, where in ((0, above, below, me - 2), (1, below, above, me + 2)):
-            @pl.when(source)
+    ways = ((0, above, below, me - 2), (1, below, above, me + 2))
+
+    def tell_on(i, where):
+        pl.semaphore_signal(chain.at[i], inc=1, device_id=(where, tp), device_id_type=MESH)
+
+    if cap:
+        for i, source, target, where in ways:
+            @pl.when(jnp.logical_and(jnp.logical_not(source), target))
             def _():
-                pl.semaphore_wait(chain.at[side_sem], 1)
-            @pl.when(target)
-            def _():
-                pl.semaphore_signal(chain.at[side_sem], inc=1, device_id=(where, tp), device_id_type=MESH)
+                tell_on(i, where)
 
     if cap:
         choices, tokens = ids_ref.shape
@@ -252,8 +256,8 @@
         blend[...] = chosen.astype(jnp.bfloat16)
         weight = weight.T
         coarse = weight.astype(jnp.bfloat16)
-        blend_hi[...] = coarse
-        blend_lo[...] = (weight - coarse.astype(jnp.float32)).astype(jnp.bfloat16)
+        blend_back[:tokens] = coarse
+        blend_back[tokens:] = (weight - coarse.astype(jnp.float32)).astype(jnp.bfloat16)
 
     def walk(d, _):
         z = zi - d
@@ -271,6 +275,12 @@
             for c in range(HALVES):
                 y_arrival(z + 1, c).wait_recv()
             fold(2 * (z + 1) + 1 - y, False)
+        if cap:
+            @pl.when((d == 1) & below & above)
+            def _():
+                for i, _, _, where in ways:
+                    pl.semaphore_wait(chain.at[i], 1)
+                    tell_on(i, where)
         return 0
 
     lax.fori_loop(1, jnp.where(zi + y > 0, zi + 2, 1), walk, 0)
@@ -297,11 +307,11 @@
 
     def near_copy(q):
         cols = pl.ds(q * span, span)
-        return remote(near_part.at[:, cols], near_got.at[:, cols], p_send.at[0, q], p_recv.at[0, q], near)
+        return remote(near_part.at[:, cols], near_got.at[:, cols], p_send.at[0], p_recv.at[0, q], near)
 
     def far_copy(q):
         cols = pl.ds(q * span, span)
-        return remote(far_part.at[:, cols], far_got.at[:, cols], p_send.at[1, q], p_recv.at[1, q], far)
+        return remote(far_part.at[:, cols], far_got.at[:, cols], p_send.at[1], p_recv.at[1, q], far)
 
     away = 1 - side
     other = picked(2 * away + 1 - core, 2 * side + 1 - core)
@@ -337,9 +347,8 @@
     ).astype(jnp.bfloat16)
 
     def finish_attention():
-        for q in range(PARTS):
-            near_copy(q).wait_send()
-            far_copy(q).wait_send()
+        remote(near_part, near_got, p_send.at[0], p_recv.at[0, 0], near).wait_send()
+        remote(far_part, far_got, p_send.at[1], p_recv.at[1, 0], far).wait_send()
 
         for c in range(HALVES):
             @pl.when(y == 0)
@@ -365,20 +374,23 @@
         return
 
     def d_copy(s):
-        return remote(send.at[s], rows_in.at[me], d_send.at[s], d_recv.at[me], (s, tp))
-
-    def d_arrival(s):
-        return remote(send.at[s], rows_in.at[s], d_send.at[s], d_recv.at[s], (s, tp))
+        return remote(send.at[s], rows_in.at[me], d_send.at[0], d_recv.at[zi], (s, tp))
+
+    def d_arrival(first, count):
+        some = pl.ds(first, count)
+        return remote(send.at[some], rows_in.at[some], d_send.at[0], d_recv.at[first // 2], (pair, tp))
 
     def r_copy(j, s):
         first, count = DOWN[j]
         w = pl.ds(first, count)
-        return remote(ret.at[w, s], back.at[w, me], r_send.at[j, s], r_recv.at[j, me], (s, tp))
-
-    def r_arrival(j, s):
+        return remote(ret.at[w, s], back.at[w, me], r_send.at[0], r_recv.at[j], (s, tp))
+
+    others = pl.ds(0, n - 1)
+
+    def r_arrival(j):
         first, count = DOWN[j]
         w = pl.ds(first, count)
-        return remote(ret.at[w, s], back.at[w, s], r_send.at[j, s], r_recv.at[j, s], (s, tp))
+        return remote(ret.at[w, others], back.at[w, others], r_send.at[0], r_recv.at[j], (pair, tp))
 
     def dispatch(d, _):
         z = d
@@ -397,6 +409,10 @@
                 rows_in[me] = got[j * cap:(j + 1) * cap]
         return 0
 
+    for i, source, target, _ in ways:
+        @pl.when(jnp.logical_and(source, jnp.logical_not(target)))
+        def _():
+            pl.semaphore_wait(chain.at[i], 1)
     lax.fori_loop(0, nz, dispatch, 0)
 
     def pass_on(p, _):
@@ -405,8 +421,7 @@
         return 0
 
     lax.fori_loop(0, DEEP, pass_on, 0)
-    for i in range(3):
-        w_copy(i).wait_recv()
+    remote(third(0), third(ff), w_send.at[0], w_recv.at[0], near).wait_recv()
     local = 2 * ff
 
     def gated(x, cols):
@@ -416,11 +431,12 @@
 
     def work(z, _):
         lax.fori_loop(DEEP + z * (DEEP // nz), DEEP + (z + 1) * (DEEP // nz), pass_on, 0)
-        for j in range(2):
-            s = 2 * z + j
-            @pl.when(s != me)
-            def _():
-                d_arrival(s).wait_recv()
+        @pl.when(z != zi)
+        def _():
+            d_arrival(2 * z, 2).wait_recv()
+        @pl.when(z == zi)
+        def _():
+            d_arrival(pair, 1).wait_recv()
         x = rows_in[pl.ds(2 * z, 2)].reshape(2 * cap, d_model)
         base = pl.multiple_of(2 * z * cap, 2 * cap)
         hid[pl.ds(base, 2 * cap), :local] = gated(x, slice(0, local))
@@ -428,11 +444,8 @@
 
     lax.fori_loop(0, nz, work, 0)
 
-    def relayed(p, _):
-        relay(p).wait_recv()
-        return 0
-
-    lax.fori_loop(0, 2 * DEEP, relayed, 0)
+    ends = gu.at[:, :, pl.ds(3 * ff, ff)]
+    remote(ends, ends, g_send.at[0], g_recv.at[0], near).wait_recv()
     hid[:, local:] = gated(rows_in[...].reshape(n * cap, d_model), slice(local, 2 * local))
 
     def give_back(j):
@@ -449,60 +462,37 @@
 
         def one(d, _):
             for k in range(2):
-                s = 2 * lax.rem(zi + d, nz) + k
+                s = 2 * jnp.where(zi >= nz // 2, d, nz - 1 - d) + k
                 @pl.when(s != me)
                 def _():
                     r_copy(j, s).start()
             return 0
 
-        lax.fori_loop(1, nz + 1, one, 0)
+        lax.fori_loop(0, nz, one, 0)
 
     def collect(j):
-        def arrive(s, _):
-            @pl.when(s != me)
-            def _():
-                r_arrival(j, s).wait_recv()
-            return 0
-
-        lax.fori_loop(0, n, arrive, 0)
+        r_arrival(j).wait_recv()
         first, count = DOWN[j]
-        for c in range(first, first + count):
-            results = back[c].reshape(n * cap, wide)
-            routed = jnp.dot(blend_hi[...], results, preferred_element_type=jnp.float32)
-            routed = routed + jnp.dot(blend_lo[...], results, preferred_element_type=jnp.float32)
-            cols = slice(c * wide, (c + 1) * wide)
-            out_ref[:, cols] = (stream_out[:, cols] + routed).astype(jnp.bfloat16)
+        results = jnp.concatenate(
+            [back[c].reshape(n * cap, wide) for c in range(first, first + count)], axis=1
+        )
+        routed = jnp.dot(blend_back[...], results, preferred_element_type=jnp.float32)
+        cols = slice(first * wide, (first + count) * wide)
+        out_ref[:, cols] = (stream_out[:, cols] + routed[:tokens] + routed[tokens:]).astype(jnp.bfloat16)
 
     for j in range(len(DOWN)):
         give_back(j)
         if j > 1:
             collect(j - 2)
+    finish_attention()
+    remote(third(0), third(ff), w_send.at[0], w_recv.at[0], near).wait_send()
+    remote(third(0), third(ff), f_send.at[0], f_recv.at[0], far).wait_send()
+    remote(third(0), third(ff), g_send.at[0], g_recv.at[0], near).wait_send()
+    remote(send.at[others], rows_in.at[others], d_send.at[0], d_recv.at[0], (pair, tp)).wait_send()
+    remote(ret.at[:, others], back.at[:, others], r_send.at[0], r_recv.at[0], (pair, tp)).wait_send()
+
     for j in range(max(len(DOWN) - 2, 0), len(DOWN)):
         collect(j)
-
-    finish_attention()
-    for i in range(3):
-        w_copy(i).wait_send()
-
-    def passed(p, _):
-        far_piece(p).wait_send()
-        relay(p).wait_send()
-        return 0
-
-    lax.fori_loop(0, 2 * DEEP, passed, 0)
-    for j in range(len(DOWN)):
-        far_down(j).wait_send()
-        relay_down(j).wait_send()
-
-    def finish(s, _):
-        @pl.when(s != me)
-        def _():
-            d_copy(s).wait_send()
-            for j in range(len(DOWN)):
-                r_copy(j, s).wait_send()
-        return 0
-
-    lax.fori_loop(0, n, finish, 0)
 
 
 def layer(n, nt, cap, *args):
@@ -531,7 +521,7 @@
         pltpu.VMEM((2 * chunk, d), bf),
         pltpu.VMEM((chunk, d), bf),
         pltpu.VMEM((chunk, d), bf),
-        dma((9,)), dma((n // 2 * HALVES,)), dma((n // 2 * HALVES,)), dma((n // 2 * HALVES,)), dma((n // 2 * HALVES,)), dma((2, PARTS)), dma((2, PARTS)),
+        dma((9,)), dma((n // 2 * HALVES,)), dma((n // 2 * HALVES,)), dma((n // 2 * HALVES,)), dma((n // 2 * HALVES,)), dma((2,)), dma((2, PARTS)),
     ]
     if cap:
         ff = args[12].shape[2]
@@ -544,14 +534,16 @@
             pltpu.VMEM((2, d, nt * ff), bf),
             pltpu.VMEM((nt * ff, d), bf),
             pltpu.VMEM((n * cap, tokens), bf),
-            pltpu.VMEM((tokens, n * cap), bf),
-            pltpu.VMEM((tokens, n * cap), bf),
+            pltpu.VMEM((2 * tokens, n * cap), bf),
         ] + [pltpu.VMEM((n, cap, d), bf)] * 2 + [
             pltpu.VMEM((n * cap, nt * ff), bf),
             pltpu.VMEM((WIDE, n, cap, d // WIDE), bf),
             pltpu.VMEM((WIDE, n, cap, d // WIDE), bf),
-            pltpu.SemaphoreType.REGULAR((2,)), dma((3,)), dma((3,)), dma((3,)),
-        ] + [dma((2 * DEEP + len(DOWN),))] * 4 + [dma((n,))] * 2 + [dma((len(DOWN), n))] * 2
+            pltpu.SemaphoreType.REGULAR((2,)), dma((3,)), dma((1,)), dma((1,)),
+        ] + [
+            dma((1,)), dma((2 * DEEP + len(DOWN),)), dma((1,)), dma((1 + len(DOWN),)),
+            dma((1,)), dma((n // 2,)), dma((1,)), dma((len(DOWN),)),
+        ]
     return pl.pallas_call(
         functools.partial(layer_kernel, n, nt, cap),
         out_shape=out_shape,

time: 93.5 us -> 89.7 us (0.959)
  Pallas kernels: 92.6 us -> 88.8 us
    pallas_call x1, Pallas kernels: 92.6 us -> 88.8 us  [layer(): pl.pallas_call(functools.partial(layer_kernel, n, nt, cap), out_shape=out...]
where the time goes in v5:
time: 89.7 us; the launch traced here: 89.5 us
  Pallas kernels  88.8 us (99%)
    pallas_call x1, Pallas kernels, layer(): pl.pallas_call(functools.partial(layer_kernel, n, nt, cap), out_shape=out...  88.8 us

profile of v5, /device:TPU:1, one launch (start us, length us, event | category | flops | bytes accessed | tf_op | source)
XLA Modules:
  0.0 89.5 jit_solution(8148705415378372586)
XLA Ops:
  0.0 88.8 %layer.1 = bf16[64,2048]{1,0:T(8,128)(2,1)S(1)} custom-call(bf16[256,256]{1,0:T(8,128)(2,1)} %refs_0_.1, bf16[256,256]{1,0:T(8,128)(2,1)} %refs_1_.1, bf16[256,128]{1,0:T(8,128)(2,1)} %refs_2_.1, bf16[256,128]{1,0:T(8,128)(2,1)} %refs_3_.1, bf16[256,256]{1,0:T(8,128)(2,1)} %refs_4_.1, f32[2]{0:T(128)} %refs_5_.1, f32[1,256]{1,0:T(1,128)} %bitcast.5, ...), custom_call_target="tpu_custom_call" | custom-call | tf_op jit(solution)/shard_map/layer/pallas_call | solution.py:547
  88.8 0.7 copy.17

commit v6 on v5

--- a/solution.py
+++ b/solution.py
@@ -18,8 +18,8 @@
 MESH = pl.DeviceIdType.MESH
 LOG2E = 1.4426950408889634
 DEEP = 8
-WIDE = 8
-DOWN = ((0, 1), (1, 1), (2, 1), (3, 1), (4, 1), (5, 1), (6, 1), (7, 1))
+WIDE = 16
+DOWN = ((0, 2), (2, 2), (4, 2), (6, 2), (8, 2), (10, 2), (12, 2), (14, 2))
 PARTS = 4
 HALVES = 2
 
@@ -51,13 +51,14 @@
     else:
         stream_out, normed_out = refs[10:12]
         refs = refs[12:]
-    kv, qs, top, total, acc, heads, ow, stream, near_part, near_got, far_part, far_got = refs[:12]
-    local_sem, z_send, z_recv, y_send, y_recv, p_send, p_recv = refs[12:19]
+    kv, qs, top, total, acc, heads, ow, stream, lam, gain, norm, near_part, near_got, far_part, far_got = refs[:15]
+    local_sem, z_send, z_recv, y_send, y_recv, p_send, p_recv = refs[15:22]
     if cap:
         (
-            stream_out, normed_out, gu, dw, blend, blend_back, send, rows_in, hid, ret, back,
-            chain, own_sem, w_send, w_recv, f_send, f_recv, g_send, g_recv, d_send, d_recv, r_send, r_recv,
-        ) = refs[19:]
+            stream_out, normed_out, gu, dw, blend, blend_back, send, rows_in, hid,
+            ids, route, chain, own_sem, w_send, w_recv, f_send, f_recv, g_send, g_recv, d_send, d_recv, r_send, r_recv,
+        ) = refs[22:-2 * len(DOWN)]
+        ret, back = refs[-2 * len(DOWN):-len(DOWN)], refs[-len(DOWN):]
 
     me, tp = lax.axis_index("sp"), lax.axis_index("tp")
     nz = n // 2
@@ -83,9 +84,17 @@
         for h in range(2)
     ]
     stream_load = pltpu.make_async_copy(stream_ref, stream, local_sem.at[8])
+    small = [(lam_ref, lam), (gain_ref, gain), (norm_ref, norm)]
+    if cap:
+        small = small + [(ids_ref, ids), (route_ref, route)]
+    small_loads = [
+        pltpu.make_async_copy(ref, held, local_sem.at[9 + i]) for i, (ref, held) in enumerate(small)
+    ]
     for load in loads + rest:
         load.start()
     stream_load.start()
+    for load in small_loads:
+        load.start()
     if cap:
         ff = gw_ref.shape[2]
 
@@ -115,7 +124,7 @@
             return remote(piece(p, 0), piece(p, 2), f_send.at[0], f_recv.at[p], far)
 
         def relay(p):
-            return remote(piece(p, 2), piece(p, 3), g_send.at[0], g_recv.at[0], near)
+            return remote(piece(p, 2), piece(p, 3), g_send.at[0], g_recv.at[p // DEEP], near)
 
         def down_piece(j, k):
             first, count = DOWN[j]
@@ -126,7 +135,7 @@
             return remote(down_piece(j, 0), down_piece(j, 2), f_send.at[0], f_recv.at[p], far)
 
         def relay_down(j):
-            return remote(down_piece(j, 2), down_piece(j, 3), g_send.at[0], g_recv.at[1 + j], near)
+            return remote(down_piece(j, 2), down_piece(j, 3), g_send.at[0], g_recv.at[2 + j], near)
 
         def third(k):
             return dw.at[pl.ds(k, 3 * ff), :]
@@ -191,7 +200,7 @@
         for i in range(3):
             w_copy(i).start()
 
-    for load in rest:
+    for load in rest + small_loads:
         load.wait()
 
     scale = HEAD_DIM ** (-0.5) * LOG2E
@@ -236,9 +245,9 @@
                 tell_on(i, where)
 
     if cap:
-        choices, tokens = ids_ref.shape
+        choices, tokens = ids.shape
         which = lax.broadcasted_iota(jnp.int32, (max(n, 8), tokens), 0)
-        named = [(ids_ref[k:k + 1, :] == which).astype(jnp.float32) for k in range(choices)]
+        named = [(ids[k:k + 1, :] == which).astype(jnp.float32) for k in range(choices)]
         before = lax.broadcasted_iota(jnp.int32, (tokens, tokens), 0) < lax.broadcasted_iota(
             jnp.int32, (tokens, tokens), 1
         )
@@ -250,9 +259,9 @@
         weight = jnp.zeros((n * cap, tokens), jnp.float32)
         for k in range(choices):
             rank = jnp.sum(named[k] * counts, axis=0, keepdims=True).astype(jnp.int32)
-            hit = (ids_ref[k:k + 1, :] * cap + rank) == place
+            hit = (ids[k:k + 1, :] * cap + rank) == place
             chosen = chosen + hit.astype(jnp.float32)
-            weight = weight + jnp.where(hit, route_ref[k:k + 1, :], 0.0)
+            weight = weight + jnp.where(hit, route[k:k + 1, :], 0.0)
         blend[...] = chosen.astype(jnp.bfloat16)
         weight = weight.T
         coarse = weight.astype(jnp.bfloat16)
@@ -289,10 +298,10 @@
         r = pl.ds(h * rows, rows)
         one = acc[0, r, :] / jnp.sum(total[0, r, :], axis=-1, keepdims=True)
         two = acc[1, r, :] / jnp.sum(total[1, r, :], axis=-1, keepdims=True)
-        diff = one - lam_ref[h] * two
+        diff = one - lam[:, h:h + 1] * two
         ms = jnp.mean(diff * diff, axis=-1, keepdims=True)
         heads[:, h * VAL_DIM:(h + 1) * VAL_DIM] = (
-            diff * lax.rsqrt(ms + EPS) * gain_ref[...] * OUT_SCALE
+            diff * lax.rsqrt(ms + EPS) * gain[...] * OUT_SCALE
         ).astype(jnp.bfloat16)
 
     ow_load.wait()
@@ -343,7 +352,7 @@
         stream_out[:, cols] = summed
         square = square + jnp.sum(summed * summed, axis=-1, keepdims=True)
     normed_out[...] = (
-        stream_out[...] * lax.rsqrt(square * (1.0 / d_model) + EPS) * norm_ref[...]
+        stream_out[...] * lax.rsqrt(square * (1.0 / d_model) + EPS) * norm[...]
     ).astype(jnp.bfloat16)
 
     def finish_attention():
@@ -380,17 +389,13 @@
         some = pl.ds(first, count)
         return remote(send.at[some], rows_in.at[some], d_send.at[0], d_recv.at[first // 2], (pair, tp))
 
+    others = pl.ds(0, n - 1)
+
     def r_copy(j, s):
-        first, count = DOWN[j]
-        w = pl.ds(first, count)
-        return remote(ret.at[w, s], back.at[w, me], r_send.at[0], r_recv.at[j], (s, tp))
-
-    others = pl.ds(0, n - 1)
+        return remote(ret[j].at[s], back[j].at[me], r_send.at[0], r_recv.at[j], (s, tp))
 
     def r_arrival(j):
-        first, count = DOWN[j]
-        w = pl.ds(first, count)
-        return remote(ret.at[w, others], back.at[w, others], r_send.at[0], r_recv.at[j], (pair, tp))
+        return remote(ret[j].at[others], back[j].at[others], r_send.at[0], r_recv.at[j], (pair, tp))
 
     def dispatch(d, _):
         z = d
@@ -444,9 +449,16 @@
 
     lax.fori_loop(0, nz, work, 0)
 
-    ends = gu.at[:, :, pl.ds(3 * ff, ff)]
-    remote(ends, ends, g_send.at[0], g_recv.at[0], near).wait_recv()
-    hid[:, local:] = gated(rows_in[...].reshape(n * cap, d_model), slice(local, 2 * local))
+    def through(i):
+        ends = gu.at[i, :, pl.ds(3 * ff, ff)]
+        remote(ends, ends, g_send.at[0], g_recv.at[i], near).wait_recv()
+        return jnp.dot(
+            rows_in[...].reshape(n * cap, d_model), gu[i, :, local:], preferred_element_type=jnp.float32
+        )
+
+    gate = through(0)
+    upper = through(1)
+    hid[:, local:] = (gate / (1.0 + jnp.exp(-gate)) * upper).astype(jnp.bfloat16)
 
     def give_back(j):
         far_down(j).wait_recv()
@@ -456,9 +468,8 @@
         down = jnp.dot(
             hid[...], dw[:, first * wide:(first + count) * wide], preferred_element_type=jnp.float32
         ).astype(jnp.bfloat16)
-        for c in range(count):
-            ret[first + c] = down[:, c * wide:(c + 1) * wide].reshape(n, cap, wide)
-            back[first + c, me] = ret[first + c, me]
+        ret[j][...] = down.reshape(n, cap, count * wide)
+        back[j][me] = ret[j][me]
 
         def one(d, _):
             for k in range(2):
@@ -473,9 +484,7 @@
     def collect(j):
         r_arrival(j).wait_recv()
         first, count = DOWN[j]
-        results = jnp.concatenate(
-            [back[c].reshape(n * cap, wide) for c in range(first, first + count)], axis=1
-        )
+        results = back[j][...].reshape(n * cap, count * wide)
         routed = jnp.dot(blend_back[...], results, preferred_element_type=jnp.float32)
         cols = slice(first * wide, (first + count) * wide)
         out_ref[:, cols] = (stream_out[:, cols] + routed[:tokens] + routed[tokens:]).astype(jnp.bfloat16)
@@ -489,7 +498,7 @@
     remote(third(0), third(ff), f_send.at[0], f_recv.at[0], far).wait_send()
     remote(third(0), third(ff), g_send.at[0], g_recv.at[0], near).wait_send()
     remote(send.at[others], rows_in.at[others], d_send.at[0], d_recv.at[0], (pair, tp)).wait_send()
-    remote(ret.at[:, others], back.at[:, others], r_send.at[0], r_recv.at[0], (pair, tp)).wait_send()
+    remote(send.at[others], rows_in.at[others], r_send.at[0], r_recv.at[0], (pair, tp)).wait_send()
 
     for j in range(max(len(DOWN) - 2, 0), len(DOWN)):
         collect(j)
@@ -501,11 +510,10 @@
     tokens, d = stream_in.shape
     vm = pl.BlockSpec(memory_space=pltpu.VMEM)
     hbm = pl.BlockSpec(memory_space=pl.ANY)
-    sm = pl.BlockSpec(memory_space=pltpu.SMEM)
     chunk = rows // nt
     dma = pltpu.SemaphoreType.DMA
     bf, f32 = jnp.bfloat16, jnp.float32
-    in_specs = [hbm, hbm, hbm, hbm, hbm, sm, vm, hbm, hbm, vm]
+    in_specs = [hbm] * 10
     out_shape = (jax.ShapeDtypeStruct((tokens, d), f32), jax.ShapeDtypeStruct((tokens, d), bf))
     out_specs = (vm, vm)
     scratch = [
@@ -517,15 +525,18 @@
         pltpu.VMEM((rows, 2 * VAL_DIM), bf),
         pltpu.VMEM(ow.shape, bf),
         pltpu.VMEM((tokens, d), bf),
+        pltpu.VMEM(args[5].shape, f32),
+        pltpu.VMEM(args[6].shape, f32),
+        pltpu.VMEM(args[9].shape, f32),
         pltpu.VMEM((2 * chunk, d), bf),
         pltpu.VMEM((2 * chunk, d), bf),
         pltpu.VMEM((chunk, d), bf),
         pltpu.VMEM((chunk, d), bf),
-        dma((9,)), dma((n // 2 * HALVES,)), dma((n // 2 * HALVES,)), dma((n // 2 * HALVES,)), dma((n // 2 * HALVES,)), dma((2,)), dma((2, PARTS)),
+        dma((14,)), dma((n // 2 * HALVES,)), dma((n // 2 * HALVES,)), dma((n // 2 * HALVES,)), dma((n // 2 * HALVES,)), dma((2,)), dma((2, PARTS)),
     ]
     if cap:
         ff = args[12].shape[2]
-        in_specs = in_specs + [vm, vm, hbm, hbm, hbm]
+        in_specs = in_specs + [hbm] * 5
         out_shape = pltpu.VMEM((tokens, d), bf)
         out_specs = vm
         scratch = scratch + [
@@ -537,13 +548,13 @@
             pltpu.VMEM((2 * tokens, n * cap), bf),
         ] + [pltpu.VMEM((n, cap, d), bf)] * 2 + [
             pltpu.VMEM((n * cap, nt * ff), bf),
-            pltpu.VMEM((WIDE, n, cap, d // WIDE), bf),
-            pltpu.VMEM((WIDE, n, cap, d // WIDE), bf),
+            pltpu.VMEM(args[10].shape, jnp.int32),
+            pltpu.VMEM(args[11].shape, f32),
             pltpu.SemaphoreType.REGULAR((2,)), dma((3,)), dma((1,)), dma((1,)),
         ] + [
-            dma((1,)), dma((2 * DEEP + len(DOWN),)), dma((1,)), dma((1 + len(DOWN),)),
+            dma((1,)), dma((2 * DEEP + len(DOWN),)), dma((1,)), dma((2 + len(DOWN),)),
             dma((1,)), dma((n // 2,)), dma((1,)), dma((len(DOWN),)),
-        ]
+        ] + [pltpu.VMEM((n, cap, count * (d // WIDE)), bf) for _, count in DOWN] * 2
     return pl.pallas_call(
         functools.partial(layer_kernel, n, nt, cap),
         out_shape=out_shape,
@@ -579,7 +590,7 @@
     top_count = expert_ids.shape[1]
     slot_cap = 2 * top_count * rows_here // n
     shared = (
-        queries_one, queries_two, keys_one, keys_two, values, lambdas,
+        queries_one, queries_two, keys_one, keys_two, values, lambdas.reshape(1, -1),
         head_gain.reshape(1, -1), out_weight, stream_in, norm_gain.reshape(1, -1),
     )
     if slot_cap % 16 == 0:

time: 89.7 us -> 88.9 us (level)
  no operation moved by 1% of the time
where the time goes in v6:
time: 88.9 us; the launch traced here: 88.8 us
  Pallas kernels  88.1 us (99%)
    pallas_call x1, Pallas kernels, layer(): pl.pallas_call(functools.partial(layer_kernel, n, nt, cap), out_shape=out...  88.1 us

profile of v6, /device:TPU:1, one launch (start us, length us, event | category | flops | bytes accessed | tf_op | source)
XLA Modules:
  0.0 88.8 jit_solution(26416280957093824)
XLA Ops:
  0.0 88.1 %layer.1 = bf16[64,2048]{1,0:T(8,128)(2,1)S(1)} custom-call(bf16[256,256]{1,0:T(8,128)(2,1)} %refs_0_.1, bf16[256,256]{1,0:T(8,128)(2,1)} %refs_1_.1, bf16[256,128]{1,0:T(8,128)(2,1)} %refs_2_.1, bf16[256,128]{1,0:T(8,128)(2,1)} %refs_3_.1, bf16[256,256]{1,0:T(8,128)(2,1)} %refs_4_.1, f32[1,2]{1,0:T(1,128)} %bitcast.9, f32[1,256]{1,0:T(1,128)} %bitcast.6, ...), custom_call_target="tpu_custom_call" | custom-call | tf_op jit(solution)/shard_map/layer/pallas_call | solution.py:558
  88.1 0.7 copy.17

commit v7 on v6

--- a/solution.py
+++ b/solution.py
@@ -21,6 +21,7 @@
 WIDE = 16
 DOWN = ((0, 2), (2, 2), (4, 2), (6, 2), (8, 2), (10, 2), (12, 2), (14, 2))
 PARTS = 4
+LAG = 3
 HALVES = 2
 
 
@@ -491,8 +492,8 @@
 
     for j in range(len(DOWN)):
         give_back(j)
-        if j > 1:
-            collect(j - 2)
+        if LAG <= j < len(DOWN) - 1:
+            collect(j - LAG)
     finish_attention()
     remote(third(0), third(ff), w_send.at[0], w_recv.at[0], near).wait_send()
     remote(third(0), third(ff), f_send.at[0], f_recv.at[0], far).wait_send()
@@ -500,7 +501,7 @@
     remote(send.at[others], rows_in.at[others], d_send.at[0], d_recv.at[0], (pair, tp)).wait_send()
     remote(send.at[others], rows_in.at[others], r_send.at[0], r_recv.at[0], (pair, tp)).wait_send()
 
-    for j in range(max(len(DOWN) - 2, 0), len(DOWN)):
+    for j in range(max(len(DOWN) - 1 - LAG, 0), len(DOWN)):
         collect(j)
 
 

time: 88.9 us -> 88.9 us (level)
  no operation moved by 1% of the time
where the time goes in v7:
time: 88.9 us; the launch traced here: 88.8 us
  Pallas kernels  88.1 us (99%)
    pallas_call x1, Pallas kernels, layer(): pl.pallas_call(functools.partial(layer_kernel, n, nt, cap), out_shape=out...  88.1 us

profile of v7, /device:TPU:1, one launch (start us, length us, event | category | flops | bytes accessed | tf_op | source)
XLA Modules:
  0.0 88.8 jit_solution(6559660645032466038)
XLA Ops:
  0.0 88.1 %layer.1 = bf16[64,2048]{1,0:T(8,128)(2,1)S(1)} custom-call(bf16[256,256]{1,0:T(8,128)(2,1)} %refs_0_.1, bf16[256,256]{1,0:T(8,128)(2,1)} %refs_1_.1, bf16[256,128]{1,0:T(8,128)(2,1)} %refs_2_.1, bf16[256,128]{1,0:T(8,128)(2,1)} %refs_3_.1, bf16[256,256]{1,0:T(8,128)(2,1)} %refs_4_.1, f32[1,2]{1,0:T(1,128)} %bitcast.9, f32[1,256]{1,0:T(1,128)} %bitcast.6, ...), custom_call_target="tpu_custom_call" | custom-call | tf_op jit(solution)/shard_map/layer/pallas_call | solution.py:559
  88.1 0.7 copy.17
